TPU v7x, 512 devices: a whole 4x4x16 slice. The times are simulated.
512 devices in a mesh: sp: 32 (over z, core), tp: 16 (over y, x).
Axes of the slice: x: 4, y: 4, z: 16, core: 2. Of those that a mesh axis runs over, the one named last changes fastest.
Arguments:
- queries: bfloat16 [16384, 1024], P('sp', 'tp'), may hold values from -20 to 20
- key_vectors: bfloat16 [16384, 1024], P('sp', 'tp'), may hold values from -20 to 20
- value_vectors: bfloat16 [16384, 1024], P('sp', 'tp'), may hold values from -6 to 6
- log_gate_sums: float32 [16384, 16], P('sp', 'tp'), may hold values from -2343 to 0, as said below
- residual: bfloat16 [16384, 2048], P('sp', 'tp'), may hold values from -24 to 24
- out_weight: bfloat16 [1024, 2048], P(None, 'tp'), may hold values from -0.75 to 0.75
- norm_gain: bfloat16 [2048], replicated, may hold values from 0.099609375 to 1.8984375
- routes: int32 [16384, 2], P('sp'), may hold values from 0 to 127, all different within a row; in each aligned block of 512 rows (0 to 511, 512 to 1023, ...) at most 10 rows name the same one
- route_weight: float32 [16384, 2], P('sp'), may hold values from 0.5 to 1.5
- expert_gate: bfloat16 [128, 2048, 512], P('sp', None, 'tp'), may hold values from -0.125 to 0.125
- expert_up: bfloat16 [128, 2048, 512], P('sp', None, 'tp'), may hold values from -0.125 to 0.125
- expert_down: bfloat16 [128, 512, 2048], P('sp', None, 'tp'), may hold values from -0.25 to 0.25
- shared_gate: bfloat16 [2048, 512], P(None, 'tp'), may hold values from -0.125 to 0.125
- shared_up: bfloat16 [2048, 512], P(None, 'tp'), may hold values from -0.125 to 0.125
- shared_down: bfloat16 [512, 2048], P(None, 'tp'), may hold values from -0.25 to 0.25
Outputs:
- layer_out: bfloat16 [16384, 2048], P('sp', 'tp')
Inputs may be any that keep to these rules, and one draw needn't show every extreme that they name: `log_gate_sums`: for each head the values do not rise along the positions. `routes`: each row names 2 different experts; among the rows of one index of sp no expert is named by more than 10 rows, a bound that some block reaches.
All inputs are finite; a program needn't handle non-finite values.
Results may differ from a plain program's by a relative error of at most 0.014.
Values may be sent and summed in bfloat16 or wider, within the bound.
No kernel may reach another device: no remote copies, remote signals or barrier semaphores. Data moves between devices by JAX's collectives and lax.ppermute only.
A program may use at most 64 MiB of HBM per device.

v0:
```python
import math

import jax
import jax.numpy as jnp
from jax import lax
from jax.sharding import PartitionSpec as P

HDIM = 64


EPSILON = 1e-06


def in_one_piece(arrays, axis, dim, along):
    both = jnp.concatenate(arrays, axis=along)
    filled, at, done = (lax.all_gather(both, axis, axis=dim, tiled=True), 0, [])
    for a in arrays:
        done.append(lax.slice_in_dim(filled, at, at + a.shape[along], axis=along))
        at += a.shape[along]
    return tuple(done)


def joined_along(tiles, dim):
    lengths = list(tiles.shape[1:])
    lengths[dim] *= tiles.shape[0]
    return jnp.moveaxis(tiles, 0, dim).reshape(lengths)


def sent_to_all(array, axis):
    copies = jnp.broadcast_to(array, (lax.axis_size(axis), *array.shape))
    return lax.all_to_all(copies, axis, split_axis=0, concat_axis=0, tiled=True)


def gather_directly(array, axis, dim):
    return joined_along(sent_to_all(array, axis), dim)


def over_copies(array, axis):
    everything = sent_to_all(array, axis)
    return jnp.sum(everything, axis=0)


def silu_gate(gate_part, up_part):
    return jax.nn.silu(gate_part) * up_part


def slot_targets(routes, experts_all, capacity):
    flat_routes = routes.reshape(-1)
    onehot = (flat_routes[:, None] == jnp.arange(experts_all, dtype=jnp.int32)[None, :]).astype(
        jnp.int32
    )
    before = jnp.cumsum(onehot, axis=0) - onehot
    return flat_routes * capacity + jnp.sum(before * onehot, axis=1)


def keep_state(fold_state):
    return fold_state


def shards(
    queries,
    key_vectors,
    value_vectors,
    log_gate_sums,
    residual,
    out_weight,
    norm_gain,
    routes,
    route_weight,
    expert_gate,
    expert_up,
    expert_down,
    shared_gate,
    shared_up,
    shared_down,
):
    tok_dev = queries.shape[0]
    head_dim = HDIM
    local_heads = log_gate_sums.shape[1]
    local_width = residual.shape[1]
    model_width = norm_gain.shape[0]
    score_scale = head_dim ** (-0.5)
    seq_first = lax.axis_index("sp") * tok_dev
    query_heads = queries.reshape(tok_dev, local_heads, head_dim)
    query_pos = seq_first + jnp.arange(tok_dev, dtype=jnp.int32)
    own_gates = log_gate_sums.T
    all_gates = lax.all_gather(log_gate_sums, "sp", axis=0, tiled=True)
    initial = (
        jnp.full((local_heads, tok_dev), -1e30, jnp.float32),
        jnp.zeros((local_heads, tok_dev), jnp.float32),
        jnp.zeros((local_heads, tok_dev, head_dim), jnp.float32),
    )
    key_heads = key_vectors.reshape(tok_dev, local_heads, head_dim)
    value_heads = value_vectors.reshape(tok_dev, local_heads, head_dim)
    key_part, value_part = in_one_piece((key_heads, value_heads), "sp", 0, 1)
    part_rows = key_part.shape[0]
    block_size = math.gcd(part_rows, 512)
    key_blocks = key_part.reshape(part_rows // block_size, block_size, local_heads, head_dim)
    value_blocks = value_part.reshape(part_rows // block_size, block_size, local_heads, head_dim)

    def one_block(fold_state, inputs):
        key_block, value_block, block_number = inputs
        block_first = block_number * block_size

        def compute(old_state):
            running_max, weight_total, summed = old_state
            gate_block = lax.dynamic_slice_in_dim(all_gates, block_first, block_size, 0).T
            scores = (
                jnp.einsum(
                    "qhd,khd->hqk", query_heads, key_block, preferred_element_type=jnp.float32
                )
                * score_scale
            )
            scores = scores + own_gates[:, :, None] - gate_block[:, None, :]
            key_pos = block_first + jnp.arange(block_size, dtype=jnp.int32)
            allowed = (key_pos[None, :] <= query_pos[:, None])[None]
            newmax = jnp.maximum(running_max, jnp.max(jnp.where(allowed, scores, -jnp.inf), axis=2))
            factor = jnp.exp(running_max - newmax)
            weight = jnp.where(allowed, jnp.exp(scores - newmax[:, :, None]), 0.0)
            weight_total = weight_total * factor + jnp.sum(weight, axis=2)
            summed = summed * factor[:, :, None] + jnp.einsum(
                "hqk,khd->hqd",
                weight.astype(jnp.bfloat16),
                value_block,
                preferred_element_type=jnp.float32,
            )
            return (newmax, weight_total, summed)

        useful = block_first <= seq_first + tok_dev - 1
        return (lax.cond(useful, compute, keep_state, fold_state), None)

    numbers = jnp.arange(part_rows // block_size, dtype=jnp.int32)
    result_state, _ = lax.scan(one_block, initial, (key_blocks, value_blocks, numbers))
    running_max, weight_total, summed = result_state
    attended = (summed / weight_total[:, :, None]).astype(jnp.bfloat16)
    attended = attended.transpose(1, 0, 2).reshape(tok_dev, local_heads * head_dim)
    weight_rows = out_weight
    projected = jnp.dot(
        gather_directly(attended, "tp", 1), weight_rows, preferred_element_type=jnp.float32
    )
    mid = (residual.astype(jnp.float32) + projected).astype(jnp.bfloat16)
    mid_wide = mid.astype(jnp.float32)
    feature_first = lax.axis_index("tp") * local_width
    squares = over_copies(jnp.sum(mid_wide * mid_wide, axis=1), "tp")
    inverse = lax.rsqrt(squares / model_width + EPSILON)
    own_gain = lax.dynamic_slice_in_dim(norm_gain, feature_first, local_width, 0).astype(
        jnp.float32
    )
    normed_own = (mid_wide * inverse[:, None] * own_gain[None, :]).astype(jnp.bfloat16)
    normed = gather_directly(normed_own, "tp", 1)
    shared_mid = silu_gate(
        jnp.dot(normed, shared_gate, preferred_element_type=jnp.float32),
        jnp.dot(normed, shared_up, preferred_element_type=jnp.float32),
    ).astype(jnp.bfloat16)
    weight_rows = shared_down
    shared_out = jnp.dot(
        lax.all_gather(shared_mid, "tp", axis=1, tiled=True),
        weight_rows,
        preferred_element_type=jnp.float32,
    )
    exp_dev = expert_gate.shape[0]
    sp_count = lax.axis_size("sp")
    experts_all = exp_dev * sp_count
    top_count = routes.shape[1]
    capacity = 5 * tok_dev * top_count // (4 * experts_all)
    targets = slot_targets(routes, experts_all, capacity)
    owners = (
        jnp.full((experts_all * capacity,), tok_dev, jnp.int32)
        .at[targets]
        .set(jnp.arange(tok_dev * top_count, dtype=jnp.int32) // top_count)
    )
    padded = jnp.concatenate(
        [normed_own, jnp.zeros((1, normed_own.shape[1]), jnp.bfloat16)], axis=0
    )
    outgoing = padded[owners].reshape(sp_count, exp_dev, capacity, normed_own.shape[1])
    rows_all = lax.all_gather(
        lax.all_to_all(outgoing, "sp", split_axis=0, concat_axis=0, tiled=True),
        "tp",
        axis=3,
        tiled=True,
    )
    gate_part = jnp.einsum(
        "secd,edf->secf", rows_all, expert_gate, preferred_element_type=jnp.float32
    )
    up_part = jnp.einsum("secd,edf->secf", rows_all, expert_up, preferred_element_type=jnp.float32)
    hidden = silu_gate(gate_part, up_part).astype(jnp.bfloat16)
    hidden_all = gather_directly(hidden, "tp", 3)
    produced = jnp.einsum(
        "secf,efd->secd", hidden_all, expert_down, preferred_element_type=jnp.float32
    ).astype(jnp.bfloat16)
    returned = lax.all_to_all(produced, "sp", split_axis=0, concat_axis=0, tiled=True)
    returned_flat = returned.reshape(experts_all * capacity, local_width)
    picked = returned_flat[targets].astype(jnp.float32).reshape(tok_dev, top_count, local_width)
    routed = jnp.sum(picked * route_weight[:, :, None], axis=1)
    return (mid_wide + shared_out + routed).astype(jnp.bfloat16)


def solution(mesh):
    placed = (
        P("sp", "tp"),
        P("sp", "tp"),
        P("sp", "tp"),
        P("sp", "tp"),
        P("sp", "tp"),
        P(None, "tp"),
        P(),
        P("sp", None),
        P("sp", None),
        P("sp", None, "tp"),
        P("sp", None, "tp"),
        P("sp", None, "tp"),
        P(None, "tp"),
        P(None, "tp"),
        P(None, "tp"),
    )
    return jax.shard_map(
        shards, mesh=mesh, in_specs=placed, out_specs=P("sp", "tp"), check_vma=False
    )
```

profile of v0, /device:TPU:1, one launch (start us, length us, event | category | flops | bytes accessed | tf_op | source)
XLA Modules:
  0.0 489.2 jit_solution(2940403956012515692)
XLA Ops:
  6.5 1.6 pad_maximum_fusion
  8.2 0.8 copy.77
  9.9 37.8 %all_gather.13 = f32[16384,1]{0,1:T(1,128)S(1)} all-gather(f32[512,1]{0,1:T(1,128)S(1)} %copy-done.8), channel_id=1, replica_groups=mesh['sp'=32,'tp'=16] {'sp'}, dimensions={0}, use_global_device_ids=true | all-gather | bytes 67584 | tf_op jit(solution)/shard_map/all_gather | solution.py:87
  47.6 41.1 %all-gather.3.cloned.1.call-done = bf16[16384,2,64]{0,2,1:T(8,128)(2,1)} async-done(((bf16[512,2,64]{0,2,1:T(8,128)(2,1)}), bf16[16384,2,64]{0,2,1:T(8,128)(2,1)}) %all-gather.3.cloned.1.call-update) | async-done | bytes 4194320 | tf_op jit(solution)/shard_map/all_gather | solution.py:16
  88.7 2.6 fusion.45
  91.3 2.5 copy_bitcast_fusion
  93.8 47.0 %while.17 = (s32[]{:T(128)}, f32[1,512]{1,0:T(1,128)S(1)}, f32[1,512]{1,0:T(1,128)S(1)}, f32[1,512,64]{1,2,0:T(8,128)S(1)}, s32[32]{0:T(128)S(1)}, /*index=5*/s3...) while((s32[]{:T(128)}, f32[1,512]{1,0:T(1,128)S(1)}, ...), condition=%wide.region_5.6_spmd.clone, body=%wide.region_0.5_spmd.clone.sunk | while | flops 70846464 | bytes 3667313 | solution.py:133
  93.9 0.6 dynamic_slice.48
  95.1 2.9 conditional.3
  95.2 1.3 fusion.6
  96.8 1.2 fusion.5
  99.2 2.9 conditional.3
  99.4 1.3 fusion.6
  100.9 1.2 fusion.5
  121.5 0.6 dynamic_slice.48
  140.9 1.1 broadcast_in_dim.50
  141.9 6.5 %all-to-all-start = ((bf16[16,512,64]{1,2,0:T(8,128)(2,1)}), bf16[16,512,64]{1,2,0:T(8,128)(2,1)S(1)}, u32[]{:S(2)}, u32[]{:S(2)}) async-start(bf16[16,512,64]{1,2,0:T(8,128)(2,1)} %broadcast_in_dim.50), calls=%async_computation | async-start | bytes 2097152 | tf_op jit(solution)/shard_map/all_to_all | solution.py:31
  149.2 4.3 scatter_custom_fusion
  153.5 11.0 %all-to-all-done = bf16[16,512,64]{1,2,0:T(8,128)(2,1)S(1)} async-done(((bf16[16,512,64]{1,2,0:T(8,128)(2,1)}), bf16[16,512,64]{1,2,0:T(8,128)(2,1)S(1)}, u32[]{:S(2)}, u32[]{:S(2)}) %all-to-all-start) | async-done | bytes 1048608 | tf_op jit(solution)/shard_map/all_to_all | solution.py:31
  165.0 0.6 broadcast_in_dim.51
  165.7 3.5 all-to-all-start.1
  169.2 0.8 dynamic-slice_convert_fusion
  170.0 5.8 %all-to-all-done.1 = f32[16,1,512]{2,1,0:T(1,128)S(1)} async-done(((f32[16,1,512]{2,1,0:T(1,128)}), f32[16,1,512]{2,1,0:T(1,128)S(1)}, u32[]{:S(2)}, u32[]{:S(2)}) %all-to-all-start.1) | async-done | bytes 32800 | tf_op jit(solution)/shard_map/all_to_all | solution.py:31
  176.0 2.8 gather_fusion
  179.1 114.7 %all_to_all.31 = bf16[32,4,10,128]{3,1,2,0:T(4,128)(2,1)S(1)} all-to-all(bf16[32,4,10,128]{3,1,2,0:T(4,128)(2,1)S(1)} %copy.81), channel_id=1, replica_groups=mesh['sp'=32,'tp'=16] {'sp'}, dimensions={0} | all-to-all | bytes 655360 | tf_op jit(solution)/shard_map/all_to_all | solution.py:177
  293.8 0.8 copy.82
  294.6 63.5 %all-gather.5.cloned.1.call-done = bf16[32,4,10,2048]{3,0,2,1:T(8,128)(2,1)} async-done(((bf16[32,4,10,128]{3,0,2,1:T(8,128)(2,1)}), bf16[32,4,10,2048]{3,0,2,1:T(8,128)(2,1)}) %all-gather.5.cloned.1.call-update) | async-done | bytes 5242896 | tf_op jit(solution)/shard_map/all_gather | solution.py:176
  358.1 4.1 convolution_bitcast_fusion.2
  362.3 1.5 fusion.23
  363.8 3.6 broadcast_bitcast_fusion
  367.4 8.3 %reshape.202 = bf16[16,2,20480]{2,1,0:T(2,128)(2,1)} reshape(bf16[16,4,10,32,32]{4,3,2,1,0:T(8,128)(2,1)} %broadcast_bitcast_fusion) | data formatting | bytes 2621440
  375.7 4.7 all-to-all-start.4
  380.5 17.4 %all-to-all-done.4 = bf16[16,2,20480]{2,1,0:T(2,128)(2,1)S(1)} async-done(((bf16[16,2,20480]{2,1,0:T(2,128)(2,1)}), bf16[16,2,20480]{2,1,0:T(2,128)(2,1)S(1)}, u32[]{:S(2)}, u32[]{:S(2)}) %all-to-all-start.4) | async-done | bytes 1310752 | tf_op jit(solution)/shard_map/all_to_all | solution.py:31
  397.9 1.7 broadcast_in_dim.52
  399.7 5.5 %all-to-all-start.2 = ((bf16[16,512,128]{1,2,0:T(8,128)(2,1)}), bf16[16,512,128]{1,2,0:T(8,128)(2,1)S(1)}, u32[]{:S(2)}, u32[]{:S(2)}) async-start(bf16[16,512,128]{1,2,0:T(8,128)(2,1)} %broadcast_in_dim.52), calls=%async_computation.2 | async-start | bytes 4194304 | tf_op jit(solution)/shard_map/all_to_all | solution.py:31
  405.2 7.2 %reshape.203 = bf16[16,4,10,32,32]{4,3,2,1,0:T(8,128)(2,1)} reshape(bf16[16,2,20480]{2,1,0:T(2,128)(2,1)} %copy-done.1) | data formatting | bytes 2621440
  412.4 3.8 bitcast_bitcast_fusion
  416.2 8.4 %copy.83 = bf16[32,4,10,16,32]{4,3,0,2,1:T(8,128)(2,1)} copy(bf16[32,4,10,16,32]{4,0,2,1,3:T(8,128)(2,1)S(1)} %bitcast_bitcast_fusion) | data formatting | bytes 2621440 | tf_op jit(solution)/shard_map/transpose | solution.py:26
  424.6 8.0 %reshape.169 = bf16[32,4,10,512]{3,0,2,1:T(8,128)(2,1)} reshape(bf16[32,4,10,16,32]{4,3,0,2,1:T(8,128)(2,1)} %copy.83) | data formatting | bytes 2621440 | tf_op jit(solution)/shard_map/reshape | solution.py:26
  432.5 1.8 fusion.24
  434.4 1.0 copy.84
  435.4 14.7 %all-to-all-start.5 = ((bf16[32,4,10,128]{3,1,2,0:T(4,128)(2,1)}), bf16[32,4,10,128]{3,1,2,0:T(4,128)(2,1)S(1)}, u32[]{:S(2)}, u32[]{:S(2)}) async-start(bf16[32,4,10,128]{3,1,2,0:T(4,128)(2,1)} %copy.84), calls=%async_computation.5 | async-start | bytes 655360 | tf_op jit(solution)/shard_map/all_to_all | solution.py:191
  450.2 1.4 fusion.46
  452.1 20.6 %all_gather.14 = bf16[512,512]{0,1:T(8,128)(2,1)S(1)} all-gather(bf16[512,32]{0,1:T(8,128)(2,1)S(1)} %fusion.29), channel_id=1, replica_groups=mesh['sp'=32,'tp'=16] {'tp'}, dimensions={1}, use_global_device_ids=true | all-gather | bytes 557056 | tf_op jit(solution)/shard_map/all_gather | solution.py:157
  472.7 2.3 all-to-all-done.5
  475.3 3.2 gather_fusion.1
  478.5 2.8 fusion.30
  481.3 1.0 fusion.26
  (170 shorter events, 22.5 us)
Async XLA Ops:
  6.5 426.0 %copy-start = (bf16[4,512,128]{2,1,0:T(8,128)(2,1)S(1)}, bf16[4,512,128]{2,1,0:T(8,128)(2,1)}, u32[]{:S(2)}) copy-start(bf16[4,512,128]{2,1,0:T(8,128)(2,1)} %param.30) | copy-start | bytes 1572868
  6.5 3.3 copy-start.8
  6.5 82.2 %all-gather.3.cloned.1.call-start = ((), (), s32[]{:S(2)}) async-start(), calls=%async_computation.6 | async-start | bytes 4325376 | tf_op jit(solution)/shard_map/all_gather | solution.py:16
  91.3 2.5 copy-start.12
  140.8 7.6 %copy-start.6 = (s32[512,2]{0,1:T(2,128)S(1)}, s32[512,2]{0,1:T(2,128)}, u32[]{:S(2)}) copy-start(s32[512,2]{0,1:T(2,128)} %param.26) | copy-start | bytes 12292
  140.8 23.6 %copy-start.2 = (bf16[1024,128]{1,0:T(8,128)(2,1)S(1)}, bf16[1024,128]{1,0:T(8,128)(2,1)}, u32[]{:S(2)}) copy-start(bf16[1024,128]{1,0:T(8,128)(2,1)} %param.24) | copy-start | bytes 786436
  140.9 23.6 %copy-start.5 = (bf16[512,128]{1,0:T(8,128)(2,1)S(1)}, bf16[512,128]{1,0:T(8,128)(2,1)}, u32[]{:S(2)}) copy-start(bf16[512,128]{1,0:T(8,128)(2,1)} %param.23) | copy-start | bytes 393220
  141.9 22.5 %all-to-all-start = ((bf16[16,512,64]{1,2,0:T(8,128)(2,1)}), bf16[16,512,64]{1,2,0:T(8,128)(2,1)S(1)}, u32[]{:S(2)}, u32[]{:S(2)}) async-start(bf16[16,512,64]{1,2,0:T(8,128)(2,1)} %broadcast_in_dim.50), calls=%async_computation | async-start | bytes 2097152 | tf_op jit(solution)/shard_map/all_to_all | solution.py:31
  165.7 10.1 %all-to-all-start.1 = ((f32[16,1,512]{2,1,0:T(1,128)}), f32[16,1,512]{2,1,0:T(1,128)S(1)}, u32[]{:S(2)}, u32[]{:S(2)}) async-start(f32[16,1,512]{2,1,0:T(1,128)} %broadcast_in_dim.51), calls=%async_computation.1 | async-start | bytes 65536 | tf_op jit(solution)/shard_map/all_to_all | solution.py:31
  169.2 188.9 %all-gather.5.cloned.1.call-start = ((), (), s32[]{:S(2)}) async-start(), calls=%async_computation.7 | async-start | bytes 5570560 | tf_op jit(solution)/shard_map/all_gather | solution.py:176
  178.8 179.3 %copy-start.10 = (bf16[4,2048,32]{1,2,0:T(8,128)(2,1)S(1)}, bf16[4,2048,32]{1,2,0:T(8,128)(2,1)}, u32[]{:S(2)}) copy-start(bf16[4,2048,32]{1,2,0:T(8,128)(2,1)} %param.28) | copy-start | bytes 1572868
  294.6 67.7 %copy-start.11 = (bf16[4,2048,32]{1,2,0:T(8,128)(2,1)S(1)}, bf16[4,2048,32]{1,2,0:T(8,128)(2,1)}, u32[]{:S(2)}) copy-start(bf16[4,2048,32]{1,2,0:T(8,128)(2,1)} %param.29) | copy-start | bytes 1572868
  358.1 4.2 copy-start.9
  375.7 22.2 %all-to-all-start.4 = ((bf16[16,2,20480]{2,1,0:T(2,128)(2,1)}), bf16[16,2,20480]{2,1,0:T(2,128)(2,1)S(1)}, u32[]{:S(2)}, u32[]{:S(2)}) async-start(bf16[16,2,20480]{2,1,0:T(2,128)(2,1)} %reshape.202), calls=%async_computation.4 | async-start | bytes 2621440 | tf_op jit(solution)/shard_map/all_to_all | solution.py:31
  397.9 1.8 copy-start.1
  399.7 35.7 %all-to-all-start.2 = ((bf16[16,512,128]{1,2,0:T(8,128)(2,1)}), bf16[16,512,128]{1,2,0:T(8,128)(2,1)S(1)}, u32[]{:S(2)}, u32[]{:S(2)}) async-start(bf16[16,512,128]{1,2,0:T(8,128)(2,1)} %broadcast_in_dim.52), calls=%async_computation.2 | async-start | bytes 4194304 | tf_op jit(solution)/shard_map/all_to_all | solution.py:31
  432.5 17.5 %copy-start.7 = (f32[512,2]{0,1:T(2,128)S(1)}, f32[512,2]{0,1:T(2,128)}, u32[]{:S(2)}) copy-start(f32[512,2]{0,1:T(2,128)} %param.27) | copy-start | bytes 12292
  435.4 39.7 %all-to-all-start.5 = ((bf16[32,4,10,128]{3,1,2,0:T(4,128)(2,1)}), bf16[32,4,10,128]{3,1,2,0:T(4,128)(2,1)S(1)}, u32[]{:S(2)}, u32[]{:S(2)}) async-start(bf16[32,4,10,128]{3,1,2,0:T(4,128)(2,1)} %copy.84), calls=%async_computation.5 | async-start | bytes 655360 | tf_op jit(solution)/shard_map/all_to_all | solution.py:191
  450.2 1.4 copy-start.3
  475.2 6.2 %copy-start.4 = (bf16[512,128]{1,0:T(8,128)(2,1)S(1)}, bf16[512,128]{1,0:T(8,128)(2,1)}, u32[]{:S(2)}) copy-start(bf16[512,128]{1,0:T(8,128)(2,1)} %param.33) | copy-start | bytes 393220
Sparse Core Ops, SparseCore 0:
  9.5 79.2 all-gather.2
  294.7 63.3 all-gather.4
where the time goes:
time: 494 us; the launch traced here: 489 us
  blocking collectives  173 us (35%)
  waiting for transfers between devices  141 us (29%)
  local copies, waits for them, and re-layouts  81.5 us (16%)
  starting transfers between devices  34.8 us (7%)
  loops' own time  22.5 us (5%)
  matrix products  15.8 us (3%)
  between operations  13.9 us (3%)
  other arithmetic  6.57 us (1%)
    all_to_all x1, blocking collectives, shards(): lax.all_to_all(outgoing, 'sp', split_axis=0, concat_axis=0, tiled=True)  115 us
    all_gather x1, waiting for transfers between devices, shards(): lax.all_gather(lax.all_to_all(outgoing, 'sp', split_axis=0, concat_axis=0...  63.5 us
    all_gather x1, waiting for transfers between devices, in_one_piece(): filled, at, done = (lax.all_gather(both, axis, axis=dim, tiled=True), 0, [])  41.1 us
    all_gather x1, blocking collectives, shards(): all_gates = lax.all_gather(log_gate_sums, 'sp', axis=0, tiled=True)  37.8 us
    all_to_all x4, waiting for transfers between devices, sent_to_all(): return lax.all_to_all(copies, axis, split_axis=0, concat_axis=0, tiled=True)  34.2 us
    unnamed x32, local copies, waits for them, and re-layouts  22.7 us
    another operation x1, loops' own time, shards(): lax.scan(one_block, initial, (key_blocks, value_blocks, numbers))  22.1 us
    all_gather x1, blocking collectives, shards(): lax.all_gather(shared_mid, 'tp', axis=1, tiled=True)  20.6 us
  transfers between devices with their start and end apart: 7, of which 6 were waited for; matrix products, arithmetic and copies ran while one was open for 8% of the time, Pallas kernels for 0%

commit v1 on v0

v1 whole, which is shorter than its diff:
```python
import jax
import jax.numpy as jnp
from jax import lax
from jax.experimental import pallas as pl
from jax.experimental.pallas import tpu as pltpu
from jax.sharding import Mesh, PartitionSpec as P

HDIM = 64
EPSILON = 1e-06
CAPACITY = 10
BF = jnp.bfloat16
F32 = jnp.float32
NN = (((1,), (0,)), ((), ()))
NT = (((1,), (1,)), ((), ()))
TN = (((0,), (0,)), ((), ()))


def dot(a, b, dims=NN):
    return lax.dot_general(a, b, dims, preferred_element_type=F32)


def call(kernel, outs, *args, smem=0, scratch=(), flops=2**28, nbytes=2**22):
    specs = [pl.BlockSpec(memory_space=pltpu.SMEM)] * smem
    specs += [pl.BlockSpec(memory_space=pltpu.VMEM)] * (len(args) - smem)
    return pl.pallas_call(
        kernel,
        out_shape=outs,
        in_specs=specs,
        out_specs=jax.tree.map(lambda _: pl.BlockSpec(memory_space=pltpu.VMEM), outs),
        scratch_shapes=scratch,
        cost_estimate=pl.CostEstimate(flops=flops, bytes_accessed=nbytes, transcendentals=0),
    )(*args)


def shape(dims, dtype=BF):
    return jax.ShapeDtypeStruct(dims, dtype)


def fold(block, query, top, acc, mask=None):
    scores = dot(block[0:72], query, TN)
    if mask is not None:
        scores = jnp.where(mask, scores, -1e30)
    new_top = jnp.maximum(top, jnp.max(scores, axis=0, keepdims=True))
    weight = jnp.exp(scores - new_top).astype(BF)
    acc = acc * jnp.exp(top - new_top) + dot(block[64:136], weight)
    return new_top, acc


def own_kernel(block_ref, query_ref, top_ref, acc_ref):
    tokens = query_ref.shape[1]
    half = tokens // 2
    for part in range(2):
        cols = slice(part * half, (part + 1) * half)
        keys = (part + 1) * half
        key_at = lax.broadcasted_iota(jnp.int32, (keys, half), 0)
        query_at = lax.broadcasted_iota(jnp.int32, (keys, half), 1) + part * half
        top, acc = fold(
            block_ref[:, 0:keys],
            query_ref[:, cols],
            jnp.full((1, half), -1e30, F32),
            jnp.zeros((72, half), F32),
            key_at <= query_at,
        )
        top_ref[:, cols] = top
        acc_ref[:, cols] = acc


def past_kernel(last, count_ref, blocks_ref, query_ref, top_in, acc_in, *out_refs):
    tokens = query_ref.shape[1]
    half = tokens // 2
    if last:
        out_ref, top_ref, acc_ref = out_refs
    else:
        top_ref, acc_ref = out_refs
    top_ref[...] = top_in[...]
    acc_ref[...] = acc_in[...]

    def step(at, carry):
        block = blocks_ref[at]
        for part in range(2):
            cols = slice(part * half, (part + 1) * half)
            top, acc = fold(block, query_ref[:, cols], top_ref[:, cols], acc_ref[:, cols])
            top_ref[:, cols] = top
            acc_ref[:, cols] = acc
        return carry

    lax.fori_loop(0, count_ref[0], step, 0)
    if last:
        out_ref[...] = (acc_ref[8:72] / acc_ref[3:4]).astype(BF)


def slots_kernel(routes_ref, targets_ref):
    experts, tokens = 128, routes_ref.shape[1]
    expert_at = lax.broadcasted_iota(jnp.int32, (experts, tokens), 0)
    earlier = (
        lax.broadcasted_iota(jnp.int32, (tokens, tokens), 0)
        < lax.broadcasted_iota(jnp.int32, (tokens, tokens), 1)
    ).astype(F32).astype(BF)
    used = jnp.zeros((experts, 1), F32)
    for k in range(2):
        named = routes_ref[k : k + 1] == expert_at
        hot = named.astype(F32)
        before = dot(hot.astype(BF), earlier) + used
        rank = jnp.sum(jnp.where(named, before, 0.0), axis=0, keepdims=True)
        targets_ref[k : k + 1] = routes_ref[k : k + 1] * CAPACITY + rank.astype(jnp.int32)
        used = used + jnp.sum(hot, axis=1, keepdims=True)


def mid_kernel(heads_ref, weight_ref, residual_ref, mid_ref, squares_ref):
    projected = dot(weight_ref[...], heads_ref[...])
    mid = (residual_ref[...].astype(F32) + projected).astype(BF)
    mid_ref[...] = mid
    wide = mid.astype(F32)
    squares_ref[...] = jnp.broadcast_to(
        jnp.sum(wide * wide, axis=0, keepdims=True)[None], squares_ref.shape
    )


def hot_slots(targets_ref, k, first, rows):
    tokens = targets_ref.shape[1]
    slot_at = lax.broadcasted_iota(jnp.int32, (rows, tokens), 0) + first
    return targets_ref[k : k + 1] == slot_at


def normed_kernel(width, mid_ref, squares_ref, gain_ref, targets_ref, rows_ref, normed_ref):
    total = jnp.sum(squares_ref[...], axis=0)
    inverse = lax.rsqrt(total / width + EPSILON)
    normed = (mid_ref[...].astype(F32) * inverse * gain_ref[...]).astype(BF)
    normed_ref[...] = normed.astype(F32).T.astype(BF)
    chunk = rows_ref.shape[0] // 4
    for part in range(4):
        hot = hot_slots(targets_ref, 0, part * chunk, chunk) | hot_slots(
            targets_ref, 1, part * chunk, chunk
        )
        rows_ref[part * chunk : (part + 1) * chunk] = dot(
            hot.astype(F32).astype(BF), normed, NT
        ).astype(BF)


def sorting():
    to = lax.broadcasted_iota(jnp.int32, (320, 320), 0)
    frm = lax.broadcasted_iota(jnp.int32, (320, 320), 1)
    el = (to >= 80).astype(jnp.int32) + (to >= 160).astype(jnp.int32) + (to >= 240).astype(jnp.int32)
    within = to - el * 80
    src = jnp.zeros_like(to)
    for s in range(1, 8):
        src = src + (within >= s * 10).astype(jnp.int32)
    return (frm == src * 40 + el * 10 + within - src * 10).astype(F32).astype(BF)


def spread_kernel(arrived_ref, normed_ref, out_ref):
    order = sorting()
    for group in range(4):
        rows = dot(order, arrived_ref[group * 320 : (group + 1) * 320]).astype(BF)
        for el in range(4):
            piece = rows[el * 80 : (el + 1) * 80]
            for y in range(4):
                out_ref[y * 4 + el, group * 80 : (group + 1) * 80] = piece
    for x in range(4):
        piece = normed_ref[x * 128 : (x + 1) * 128]
        for y in range(4):
            out_ref[y * 4 + x, 320:448] = piece


def hidden_kernel(rows_ref, weight_ref, out_ref):
    expert = jnp.zeros((320, 256), F32)
    shared = jnp.zeros((128, 256), F32)

    def weights(first, cols):
        return jnp.concatenate(
            [weight_ref[x, g : g + 32, cols] for g in (first, first + 32) for x in range(4)], axis=0
        )

    for t in range(0, 16, 2):
        cols = slice(t * 128, (t + 2) * 128)
        rows = jnp.concatenate([rows_ref[t], rows_ref[t + 1]], axis=1)
        expert = expert + dot(rows[0:320], weights(0, cols), NT)
        shared = shared + dot(rows[320:448], weights(64, cols), NT)
    for first, count, both in ((0, 320, expert), (320, 128, shared)):
        gate, up = both[:, 0:128], both[:, 128:256]
        hidden = (gate / (1.0 + jnp.exp(-gate)) * up).astype(BF)
        for t in range(16):
            out_ref[t, first : first + count] = hidden


def down_kernel(hidden_ref, weight_ref, shared_ref, out_ref, shared_out_ref):
    order = sorting()
    produced = []
    for x in range(4):
        rows = jnp.zeros((320, 128), F32)
        shared = jnp.zeros((128, 128), F32)
        for y in range(0, 4, 2):
            cols = slice(y * 128, (y + 2) * 128)
            both = jnp.concatenate([hidden_ref[y * 4 + x], hidden_ref[y * 4 + 4 + x]], axis=1)
            rows = rows + dot(both[0:320], weight_ref[x, cols])
            shared = shared + dot(both[320:448], shared_ref[cols])
        produced.append(rows.astype(BF))
        shared_out_ref[x * 128 : (x + 1) * 128] = shared
    for group in range(4):
        rows = jnp.concatenate([p[group * 80 : (group + 1) * 80] for p in produced], axis=0)
        out_ref[group * 320 : (group + 1) * 320] = dot(order, rows, TN).astype(BF)


def last_kernel(returned_ref, targets_ref, weight_ref, mid_ref, shared_ref, out_ref):
    tokens = targets_ref.shape[1]
    total = mid_ref[...].astype(F32)
    slots = returned_ref.shape[0]
    chunk = slots // 5
    picked = [jnp.zeros(mid_ref.shape, F32) for _ in range(2)]
    for part in range(5):
        rows = returned_ref[part * chunk : (part + 1) * chunk]
        for k in range(2):
            hot = hot_slots(targets_ref, k, part * chunk, chunk).astype(F32).astype(BF)
            picked[k] = picked[k] + dot(rows, hot, TN)
    for k in range(2):
        total = total + picked[k] * weight_ref[k : k + 1]
    out_ref[...] = (total.T + shared_ref[...]).astype(BF)


def pieces(value):
    parts = []
    for _ in range(3):
        part = lax.reduce_precision(value, 8, 7)
        parts.append(part)
        value = value - part
    return jnp.concatenate(parts, axis=0).astype(BF)


def exchange(array, axis):
    return lax.all_to_all(array, axis, split_axis=0, concat_axis=0, tiled=True)


def shards(
    queries,
    key_vectors,
    value_vectors,
    log_gate_sums,
    residual,
    out_weight,
    norm_gain,
    routes,
    route_weight,
    expert_gate,
    expert_up,
    expert_down,
    shared_gate,
    shared_up,
    shared_down,
):
    tokens = queries.shape[0]
    width = norm_gain.shape[0]
    z, c = lax.axis_index("z"), lax.axis_index("c")
    tp = ("y", "x")
    gates = log_gate_sums.T
    ones = jnp.ones((3, tokens), BF)
    zeros = jnp.zeros((2, tokens), BF)
    block = jnp.concatenate(
        [key_vectors.T, pieces(-gates), ones, zeros, value_vectors.T], axis=0
    )
    gathered = lax.all_gather(block, "z", axis=0, tiled=False)
    query = jnp.concatenate([queries.T * BF(HDIM**-0.5), ones, pieces(gates), zeros], axis=0)
    state = (shape((1, tokens), F32), shape((72, tokens), F32))
    top, acc = call(own_kernel, state, block, query)

    local = jnp.stack([expert_gate, expert_up], axis=1).transpose(0, 1, 3, 2).reshape(4, 64, width)
    both = jnp.concatenate([shared_gate.T, shared_up.T], axis=0)
    local = jnp.concatenate([local, jnp.broadcast_to(both[None], (4, 64, width))], axis=1)
    up_weight = exchange(local, "x")
    targets = call(slots_kernel, shape((2, tokens), jnp.int32), routes.T)
    at = (lax.axis_index("y") * 4 + lax.axis_index("x")) * 128
    gain = lax.dynamic_slice_in_dim(norm_gain, at, 128, 0).astype(F32)[:, None]

    partner = lax.ppermute(gathered, "c", [(0, 1), (1, 0)])
    top, acc = call(
        lambda *refs: past_kernel(False, *refs), state, z.reshape(1), gathered, query, top, acc, smem=1
    )
    attended, _, _ = call(
        lambda *refs: past_kernel(True, *refs),
        (shape((HDIM, tokens)), *state),
        (z + c).reshape(1),
        partner,
        query,
        top,
        acc,
        smem=1,
    )
    heads = exchange(jnp.broadcast_to(attended[None], (16, HDIM, tokens)), tp)
    mid, squares = call(
        mid_kernel,
        (shape((128, tokens)), shape((16, 1, tokens), F32)),
        heads.reshape(16 * HDIM, tokens),
        out_weight.T,
        residual.T,
    )
    squares = exchange(squares, tp)
    rows, normed = call(
        lambda *refs: normed_kernel(width, *refs),
        (shape((1280, 128)), shape((tokens, 128))),
        mid,
        squares,
        gain,
        targets,
    )
    arrived = exchange(rows.reshape(32, 40, 128), ("z", "c")).reshape(1280, 128)
    spread = exchange(call(spread_kernel, shape((16, 448, 128)), arrived, normed), tp)
    hidden = exchange(call(hidden_kernel, shape((16, 448, 128)), spread, up_weight), tp)
    produced, shared = call(
        down_kernel,
        (shape((1280, 128)), shape((tokens, 128), F32)),
        hidden,
        expert_down,
        shared_down,
    )
    returned = exchange(produced.reshape(32, 40, 128), ("z", "c")).reshape(1280, 128)
    return call(
        last_kernel, shape((tokens, 128)), returned, targets, route_weight.T, mid, shared
    )


def solution(mesh):
    grid = Mesh(mesh.devices.reshape(16, 2, 4, 4), ("z", "c", "y", "x"))
    sp, tp = ("z", "c"), ("y", "x")
    placed = (
        P(sp, tp),
        P(sp, tp),
        P(sp, tp),
        P(sp, tp),
        P(sp, tp),
        P(None, tp),
        P(),
        P(sp, None),
        P(sp, None),
        P(sp, None, tp),
        P(sp, None, tp),
        P(sp, None, tp),
        P(None, tp),
        P(None, tp),
        P(None, tp),
    )
    return jax.shard_map(
        shards, mesh=grid, in_specs=placed, out_specs=P(sp, tp), check_vma=False
    )
```

time: 494 us -> 344 us (0.70)
  blocking collectives: 173 us -> 89 us
  local copies, waits for them, and re-layouts: 81.5 us -> 13.8 us
  Pallas kernels: 0 us -> 27.1 us
  starting transfers between devices: 34.8 us -> 59.3 us
  loops' own time: 22.5 us -> 0 us
  matrix products: 15.8 us -> 0 us
  waiting for transfers between devices: 141 us -> 136 us
    all_gather x2 -> x0, blocking collectives: 58.4 us -> none  [the longest x1 37.8 us: shards(): all_gates = lax.all_gather(log_gate_sums, 'sp', axis=0, tiled=True)]
    all_gather x2 -> x1, waiting for transfers between devices: 105 us -> 69.2 us  [shards(): gathered = lax.all_gather(block, 'z', axis=0, tiled=False)]
    all_to_all x5 -> x4, waiting for transfers between devices: 36.5 us -> 66.7 us  [exchange(): return lax.all_to_all(array, axis, split_axis=0, concat_axis=0, tiled=True)]
    pallas_call x0 -> x10, Pallas kernels: none -> 27.1 us  [call(): pl.pallas_call(kernel, out_shape=outs, in_specs=specs, out_specs=jax.tree...]
    all_to_all x1 -> x3, blocking collectives: 115 us -> 89 us  [exchange(): return lax.all_to_all(array, axis, split_axis=0, concat_axis=0, tiled=True)]
    another operation x33 -> x0, loops' own time: 22.5 us -> none  [the longest x1 22.1 us: shards(): lax.scan(one_block, initial, (key_blocks, value_blocks, numbers))]
    dynamic_slice x34 -> x0, local copies, waits for them, and re-layouts: 18.9 us -> none  [the longest x32 18.8 us: shards(): lax.scan(one_block, initial, (key_blocks, value_blocks, numbers))]
    unnamed x32 -> x24, local copies, waits for them, and re-layouts: 22.7 us -> 6.13 us
  transfers between devices with their start and end apart: 7 -> 6, of which waited for: 6 -> 5; matrix products, arithmetic and copies ran while one was open for 8% -> 2% of each run, Pallas kernels for 0% -> 3%
where the time goes in v1:
time: 344 us; the launch traced here: 343 us
  waiting for transfers between devices  136 us (40%)
  blocking collectives  89 us (26%)
  starting transfers between devices  59.3 us (17%)
  Pallas kernels  27.1 us (8%)
  local copies, waits for them, and re-layouts  13.8 us (4%)
  between operations  13.5 us (4%)
  other arithmetic  4.01 us (1%)
    all_to_all x3, blocking collectives, exchange(): return lax.all_to_all(array, axis, split_axis=0, concat_axis=0, tiled=True)  89 us
    all_gather x1, waiting for transfers between devices, shards(): gathered = lax.all_gather(block, 'z', axis=0, tiled=False)  69.2 us
    all_to_all x4, waiting for transfers between devices, exchange(): return lax.all_to_all(array, axis, split_axis=0, concat_axis=0, tiled=True)  66.7 us
    all_to_all x4, starting transfers between devices, exchange(): return lax.all_to_all(array, axis, split_axis=0, concat_axis=0, tiled=True)  47.4 us
    pallas_call x10, Pallas kernels, call(): pl.pallas_call(kernel, out_shape=outs, in_specs=specs, out_specs=jax.tree...  27.1 us
    ppermute x1, starting transfers between devices, shards(): partner = lax.ppermute(gathered, 'c', [(0, 1), (1, 0)])  11.9 us
  transfers between devices with their start and end apart: 6, of which 5 were waited for; matrix products, arithmetic and copies ran while one was open for 2% of the time, Pallas kernels for 3%

profile of v1, /device:TPU:1, one launch (start us, length us, event | category | flops | bytes accessed | tf_op | source)
XLA Modules:
  0.0 342.7 jit_solution(11803765823476847214)
XLA Ops:
  6.5 0.0 all-gather.3.cloned.1.call-start
  6.5 0.7 fusion.3
  7.3 3.6 %concatenate.18.block_ref = bf16[136,512]{1,0:T(8,128)(2,1)} concatenate(bf16[64,512]{1,0:T(8,128)(2,1)} %bitcast.56, bf16[1,512]{1,0:T(2,128)(2,1)S(1)} %get-tuple-element.32, bf16[1,512]{1,0:T(2,128)(2,1)S(1)} %get-tuple-element.29, bf16[1,512]{1,0:T(2,128)(2,1)S(1)} %get-tuple-element.28, bf16[3,512]{1,0:T(4,128)(2,1)S(1)} %broadcast_in_dim.23, ...), dimensions={0} | concatenate | bytes 278528 | tf_op jit(solution)/shard_map/concatenate | solution.py:257
  10.8 0.0 all-gather.3.cloned.1.call-update
  10.8 69.2 %all-gather.3.cloned.1.call-done = bf16[2176,512]{1,0:T(8,128)(2,1)} async-done(((bf16[136,512]{1,0:T(8,128)(2,1)}), bf16[2176,512]{1,0:T(8,128)(2,1)}) %all-gather.3.cloned.1.call-update) | async-done | bytes 2228240 | tf_op jit(solution)/shard_map/all_gather | solution.py:260
  80.0 11.9 %collective-permute-start = (bf16[16,136,512]{2,1,0:T(8,128)(2,1)}, bf16[16,136,512]{2,1,0:T(8,128)(2,1)S(1)}, u32[]{:S(2)}, u32[]{:S(2)}) collective-permute-start(bf16[16,136,512]{2,1,0:T(8,128)(2,1)} %bitcast.44), channel_id=1, source_target_pairs={{0,16},{16,0},{1,17},{17,1},{2,18},{18,2},{3,19},{19,3},{4,20},{20... | collective-permute-start | bytes 6684680 | tf_op jit(solution)/shard_map/ppermute | solution.py:273
  91.9 0.8 multiply_bitcast_fusion
  92.8 1.3 concatenate.19.query_ref.refs_2_
  94.0 2.2 shard_map.145
  96.2 2.4 shard_map.146
  98.6 0.0 collective-permute-done.refs_1_
  98.6 1.4 copy-done.2
  100.0 3.3 shard_map.147
  103.3 2.0 broadcast_in_dim.25
  105.3 6.5 %all-to-all-start = ((bf16[16,64,512]{2,1,0:T(8,128)(2,1)}), bf16[16,64,512]{2,1,0:T(8,128)(2,1)S(1)}, u32[]{:S(2)}, u32[]{:S(2)}) async-start(bf16[16,64,512]{2,1,0:T(8,128)(2,1)} %broadcast_in_dim.25), calls=%async_computation | async-start | bytes 2097152 | tf_op jit(solution)/shard_map/all_to_all | solution.py:230
  111.8 0.0 copy-done.6
  111.8 0.8 copy.16
  112.7 0.8 copy.17
  113.4 18.1 %all-to-all-done = bf16[16,64,512]{2,1,0:T(8,128)(2,1)S(1)} async-done(((bf16[16,64,512]{2,1,0:T(8,128)(2,1)}), bf16[16,64,512]{2,1,0:T(8,128)(2,1)S(1)}, u32[]{:S(2)}, u32[]{:S(2)}) %all-to-all-start) | async-done | bytes 1048608 | tf_op jit(solution)/shard_map/all_to_all | solution.py:230
  131.6 1.0 copy-done.1
  132.6 2.4 shard_map.148
  135.0 3.5 %all-to-all-start.1 = ((f32[16,1,512]{2,1,0:T(1,128)}), f32[16,1,512]{2,1,0:T(1,128)S(1)}, u32[]{:S(2)}, u32[]{:S(2)}) async-start(f32[16,1,512]{2,1,0:T(1,128)} %get-tuple-element.22), calls=%async_computation.1 | async-start | bytes 65536 | tf_op jit(solution)/shard_map/all_to_all | solution.py:230
  138.5 0.8 bitcast_convert_fusion
  139.2 0.7 copy.18.refs_2_
  139.9 1.6 shard_map.149.refs_3_.targets_ref
  141.6 3.3 all-to-all-done.1.refs_1_
  144.8 0.6 copy-done.10
  145.5 2.4 shard_map.150
  147.9 33.8 %all-to-all-start.2 = ((bf16[32,40,128]{2,1,0:T(8,128)(2,1)}), bf16[32,40,128]{2,1,0:T(8,128)(2,1)S(1)}, u32[]{:S(2)}, u32[]{:S(2)}) async-start(bf16[32,40,128]{2,1,0:T(8,128)(2,1)} %bitcast.51), calls=%async_computation.2 | async-start | bytes 655360 | tf_op jit(solution)/shard_map/all_to_all | solution.py:230
  181.7 0.0 copy-start.8
  181.7 0.0 copy-start.9
  181.7 0.1 maximum_bitcast_fusion
  181.8 0.1 copy.19
  181.9 0.7 copy-done.8
  182.6 0.1 copy-done.9
  182.7 0.1 broadcast_in_dim.28
  182.8 1.6 pad_maximum_fusion
  184.4 22.3 %all-to-all-done.2 = bf16[32,40,128]{2,1,0:T(8,128)(2,1)S(1)} async-done(((bf16[32,40,128]{2,1,0:T(8,128)(2,1)}), bf16[32,40,128]{2,1,0:T(8,128)(2,1)S(1)}, u32[]{:S(2)}, u32[]{:S(2)}) %all-to-all-start.2) | async-done | bytes 327712 | tf_op jit(solution)/shard_map/all_to_all | solution.py:230
  206.7 0.7 copy-done.3
  207.4 3.6 %all-to-all-start.4 = ((bf16[4,128,2048]{2,1,0:T(8,128)(2,1)}), bf16[4,128,2048]{2,1,0:T(8,128)(2,1)S(1)}, u32[]{:S(2)}, u32[]{:S(2)}) async-start(bf16[4,128,2048]{2,1,0:T(8,128)(2,1)} %pad_maximum_fusion), calls=%async_computation.4 | async-start | bytes 4194304 | tf_op jit(solution)/shard_map/all_to_all | solution.py:230
  211.0 2.7 shard_map.151
  213.7 23.0 %all-to-all-done.4.weight_ref = bf16[4,128,2048]{2,1,0:T(8,128)(2,1)S(1)} async-done(((bf16[4,128,2048]{2,1,0:T(8,128)(2,1)}), bf16[4,128,2048]{2,1,0:T(8,128)(2,1)S(1)}, u32[]{:S(2)}, u32[]{:S(2)}) %all-to-all-start.4) | async-done | bytes 2097184 | tf_op jit(solution)/shard_map/all_to_all | solution.py:230
  236.7 28.5 %all_to_all.35.rows_ref = bf16[16,448,128]{2,1,0:T(8,128)(2,1)} all-to-all(bf16[16,448,128]{2,1,0:T(8,128)(2,1)} %shard_map.151), channel_id=1, replica_groups=mesh['z'=16,'c'=2,'y'=4,'x'=4] {'y','x'}, dimensions={0} | all-to-all | bytes 3670016 | tf_op jit(solution)/shard_map/all_to_all | solution.py:230
  265.2 4.3 %shard_map.152 = bf16[16,448,128]{2,1,0:T(8,128)(2,1)} custom-call(bf16[16,448,128]{2,1,0:T(8,128)(2,1)} %all_to_all.35.rows_ref, bf16[4,128,2048]{2,1,0:T(8,128)(2,1)} %copy-done), custom_call_target="tpu_custom_call" | custom-call | flops 268435456 | bytes 4194304 | tf_op jit(solution)/shard_map/pallas_call | solution.py:25
  269.5 27.9 %all_to_all.36.hidden_ref = bf16[16,448,128]{2,1,0:T(8,128)(2,1)} all-to-all(bf16[16,448,128]{2,1,0:T(8,128)(2,1)} %shard_map.152), channel_id=1, replica_groups=mesh['z'=16,'c'=2,'y'=4,'x'=4] {'y','x'}, dimensions={0} | all-to-all | bytes 3670016 | tf_op jit(solution)/shard_map/all_to_all | solution.py:230
  297.4 3.4 shard_map.153
  300.8 32.6 %all_to_all.37 = bf16[32,40,128]{2,1,0:T(8,128)(2,1)} all-to-all(bf16[32,40,128]{2,1,0:T(8,128)(2,1)} %bitcast.53), channel_id=1, replica_groups=mesh['z'=16,'c'=2,'y'=4,'x'=4] {'z','c'}, dimensions={0} | all-to-all | bytes 655360 | tf_op jit(solution)/shard_map/all_to_all | solution.py:230
  333.4 2.5 shard_map.154
  (16 shorter events, 0.0 us)
Async XLA Ops:
  6.5 73.5 %all-gather.3.cloned.1.call-start = ((), (), s32[]{:S(2)}) async-start(), calls=%async_computation.7 | async-start | bytes 2367488 | tf_op jit(solution)/shard_map/all_gather | solution.py:260
  80.0 18.5 %collective-permute-start = (bf16[16,136,512]{2,1,0:T(8,128)(2,1)}, bf16[16,136,512]{2,1,0:T(8,128)(2,1)S(1)}, u32[]{:S(2)}, u32[]{:S(2)}) collective-permute-start(bf16[16,136,512]{2,1,0:T(8,128)(2,1)} %bitcast.44), channel_id=1, source_target_pairs={{0,16},{16,0},{1,17},{17,1},{2,18},{18,2},{3,19},{19,3},{4,20},{20... | collective-permute-start | bytes 6684680 | tf_op jit(solution)/shard_map/ppermute | solution.py:273
  98.6 1.4 copy-start.2
  103.3 8.5 %copy-start.6 = (bf16[1024,128]{1,0:T(8,128)(2,1)S(1)}, bf16[1024,128]{1,0:T(8,128)(2,1)}, u32[]{:S(2)}) copy-start(bf16[1024,128]{1,0:T(8,128)(2,1)} %param.20) | copy-start | bytes 786436
  103.3 9.4 %copy-start.7 = (bf16[512,128]{1,0:T(8,128)(2,1)S(1)}, bf16[512,128]{1,0:T(8,128)(2,1)}, u32[]{:S(2)}) copy-start(bf16[512,128]{1,0:T(8,128)(2,1)} %param.19) | copy-start | bytes 393220
  105.3 26.3 %all-to-all-start = ((bf16[16,64,512]{2,1,0:T(8,128)(2,1)}), bf16[16,64,512]{2,1,0:T(8,128)(2,1)S(1)}, u32[]{:S(2)}, u32[]{:S(2)}) async-start(bf16[16,64,512]{2,1,0:T(8,128)(2,1)} %broadcast_in_dim.25), calls=%async_computation | async-start | bytes 2097152 | tf_op jit(solution)/shard_map/all_to_all | solution.py:230
  131.6 1.0 copy-start.1
  132.6 49.1 %copy-start.4 = (bf16[4,2048,32]{1,2,0:T(8,128)(2,1)S(1)}, bf16[4,2048,32]{1,2,0:T(8,128)(2,1)}, u32[]{:S(2)}) copy-start(bf16[4,2048,32]{1,2,0:T(8,128)(2,1)} %param.25) | copy-start | bytes 1572868
  132.6 49.1 %copy-start.5 = (bf16[4,2048,32]{1,2,0:T(8,128)(2,1)S(1)}, bf16[4,2048,32]{1,2,0:T(8,128)(2,1)}, u32[]{:S(2)}) copy-start(bf16[4,2048,32]{1,2,0:T(8,128)(2,1)} %param.24) | copy-start | bytes 1572868
  135.0 9.9 %all-to-all-start.1 = ((f32[16,1,512]{2,1,0:T(1,128)}), f32[16,1,512]{2,1,0:T(1,128)S(1)}, u32[]{:S(2)}, u32[]{:S(2)}) async-start(f32[16,1,512]{2,1,0:T(1,128)} %get-tuple-element.22), calls=%async_computation.1 | async-start | bytes 65536 | tf_op jit(solution)/shard_map/all_to_all | solution.py:230
  144.8 0.6 copy-start.10
  147.9 58.8 %all-to-all-start.2 = ((bf16[32,40,128]{2,1,0:T(8,128)(2,1)}), bf16[32,40,128]{2,1,0:T(8,128)(2,1)S(1)}, u32[]{:S(2)}, u32[]{:S(2)}) async-start(bf16[32,40,128]{2,1,0:T(8,128)(2,1)} %bitcast.51), calls=%async_computation.2 | async-start | bytes 655360 | tf_op jit(solution)/shard_map/all_to_all | solution.py:230
  181.7 0.9 copy-start.8
  181.7 1.0 copy-start.9
  206.7 0.7 copy-start.3
  207.4 29.3 %all-to-all-start.4 = ((bf16[4,128,2048]{2,1,0:T(8,128)(2,1)}), bf16[4,128,2048]{2,1,0:T(8,128)(2,1)S(1)}, u32[]{:S(2)}, u32[]{:S(2)}) async-start(bf16[4,128,2048]{2,1,0:T(8,128)(2,1)} %pad_maximum_fusion), calls=%async_computation.4 | async-start | bytes 4194304 | tf_op jit(solution)/shard_map/all_to_all | solution.py:230
  236.7 28.5 %copy-start = (bf16[4,128,2048]{2,1,0:T(8,128)(2,1)}, bf16[4,128,2048]{2,1,0:T(8,128)(2,1)S(1)}, u32[]{:S(2)}) copy-start(bf16[4,128,2048]{2,1,0:T(8,128)(2,1)S(1)} %all-to-all-done.4.weight_ref) | copy-start | bytes 6291460
Sparse Core Ops, SparseCore 0:
  11.0 69.0 all-gather.2

commit v2 on v1

--- a/solution.py
+++ b/solution.py
@@ -1,3 +1,5 @@
+import functools
+
 import jax
 import jax.numpy as jnp
 from jax import lax
@@ -36,57 +38,71 @@
     return jax.ShapeDtypeStruct(dims, dtype)
 
 
-def fold(block, query, top, acc, mask=None):
-    scores = dot(block[0:72], query, TN)
-    if mask is not None:
-        scores = jnp.where(mask, scores, -1e30)
-    new_top = jnp.maximum(top, jnp.max(scores, axis=0, keepdims=True))
-    weight = jnp.exp(scores - new_top).astype(BF)
-    acc = acc * jnp.exp(top - new_top) + dot(block[64:136], weight)
-    return new_top, acc
-
-
-def own_kernel(block_ref, query_ref, top_ref, acc_ref):
-    tokens = query_ref.shape[1]
+def fold(block, query_ref, top_ref, acc_ref, parts):
+    half = query_ref.shape[1] // 4
+    columns = [slice(part * half, (part + 1) * half) for part in parts]
+    keys = block[0:72].astype(F32).T.astype(BF)
+    scores = [dot(keys, query_ref[:, cols]) for cols in columns]
+    old = [top_ref[:, cols] for cols in columns]
+    new = [jnp.maximum(o, jnp.max(s, axis=0, keepdims=True)) for o, s in zip(old, scores)]
+    weights = [jnp.exp(s - n).astype(BF) for s, n in zip(scores, new)]
+    values = [
+        acc_ref[:, cols] * jnp.exp(o - n) + dot(block[64:136], w)
+        for cols, o, n, w in zip(columns, old, new, weights)
+    ]
+    for cols, n, v in zip(columns, new, values):
+        top_ref[:, cols] = n
+        acc_ref[:, cols] = v
+
+
+def own_kernel(core_ref, block_ref, query_ref, top_ref, acc_ref):
+    tokens = block_ref.shape[1]
     half = tokens // 2
     for part in range(2):
         cols = slice(part * half, (part + 1) * half)
         keys = (part + 1) * half
         key_at = lax.broadcasted_iota(jnp.int32, (keys, half), 0)
         query_at = lax.broadcasted_iota(jnp.int32, (keys, half), 1) + part * half
-        top, acc = fold(
-            block_ref[:, 0:keys],
-            query_ref[:, cols],
-            jnp.full((1, half), -1e30, F32),
-            jnp.zeros((72, half), F32),
-            key_at <= query_at,
-        )
+        scores = dot(block_ref[0:72, 0:keys], query_ref[:, cols], TN)
+        scores = jnp.where(key_at <= query_at, scores, -1e30)
+        top = jnp.max(scores, axis=0, keepdims=True)
         top_ref[:, cols] = top
-        acc_ref[:, cols] = acc
-
-
-def past_kernel(last, count_ref, blocks_ref, query_ref, top_in, acc_in, *out_refs):
-    tokens = query_ref.shape[1]
-    half = tokens // 2
-    if last:
-        out_ref, top_ref, acc_ref = out_refs
-    else:
-        top_ref, acc_ref = out_refs
+        acc_ref[:, cols] = dot(block_ref[64:136, 0:keys], jnp.exp(scores - top).astype(BF))
+    top_ref[:, tokens:] = jnp.full((1, tokens), -1e30, F32)
+    acc_ref[:, tokens:] = jnp.zeros((72, tokens), F32)
+
+    @pl.when(core_ref[0] == 0)
+    def _():
+        fold(block_ref[...], query_ref, top_ref, acc_ref, (2, 3))
+
+
+def past_kernel(k, chips, count, chip_ref, *refs):
+    blocks, query_ref = refs[0:count], refs[count]
+    top_in, acc_in, top_ref, acc_ref = refs[1 + count : 5 + count]
     top_ref[...] = top_in[...]
     acc_ref[...] = acc_in[...]
-
-    def step(at, carry):
-        block = blocks_ref[at]
-        for part in range(2):
-            cols = slice(part * half, (part + 1) * half)
-            top, acc = fold(block, query_ref[:, cols], top_ref[:, cols], acc_ref[:, cols])
-            top_ref[:, cols] = top
-            acc_ref[:, cols] = acc
-        return carry
-
-    lax.fori_loop(0, count_ref[0], step, 0)
-    if last:
-        out_ref[...] = (acc_ref[8:72] / acc_ref[3:4]).astype(BF)
+    chip = chip_ref[0]
+    for useful, block_ref in zip((chip >= k, chip + k >= chips), blocks):
+
+        @pl.when(useful)
+        def _():
+            fold(block_ref[...], query_ref, top_ref, acc_ref, range(4))
+
+    if count == 1:
+        sent_ref = refs[5 + count]
+        tokens = sent_ref.shape[1]
+        sent_ref[0:72] = acc_ref[:, tokens:]
+        sent_ref[72:80] = jnp.broadcast_to(top_ref[:, tokens:], (8, tokens))
+
+
+def merge_kernel(top_ref, acc_ref, other_ref, out_ref):
+    tokens = out_ref.shape[2]
+    top, other = top_ref[:, 0:tokens], other_ref[72:73]
+    both = jnp.maximum(top, other)
+    acc = acc_ref[:, 0:tokens] * jnp.exp(top - both) + other_ref[0:72] * jnp.exp(other - both)
+    attended = (acc[8:72] / acc[3:4]).astype(BF)
+    for t in range(16):
+        out_ref[t] = attended
 
 
 def slots_kernel(routes_ref, targets_ref):
@@ -257,10 +273,12 @@
     block = jnp.concatenate(
         [key_vectors.T, pieces(-gates), ones, zeros, value_vectors.T], axis=0
     )
-    gathered = lax.all_gather(block, "z", axis=0, tiled=False)
     query = jnp.concatenate([queries.T * BF(HDIM**-0.5), ones, pieces(gates), zeros], axis=0)
-    state = (shape((1, tokens), F32), shape((72, tokens), F32))
-    top, acc = call(own_kernel, state, block, query)
+    query = jnp.concatenate([query, lax.ppermute(query, "c", ((0, 1), (1, 0)))], axis=1)
+    state = (shape((1, 2 * tokens), F32), shape((72, 2 * tokens), F32))
+    chips = lax.axis_size("z")
+    ahead = [(i, i + 1) for i in range(chips - 1)]
+    back = [(i, (i - 1) % chips) for i in range(chips)]
 
     local = jnp.stack([expert_gate, expert_up], axis=1).transpose(0, 1, 3, 2).reshape(4, 64, width)
     both = jnp.concatenate([shared_gate.T, shared_up.T], axis=0)
@@ -268,29 +286,42 @@
     up_weight = exchange(local, "x")
     targets = call(slots_kernel, shape((2, tokens), jnp.int32), routes.T)
     at = (lax.axis_index("y") * 4 + lax.axis_index("x")) * 128
+    out_rows, residual = out_weight.T, residual.T
     gain = lax.dynamic_slice_in_dim(norm_gain, at, 128, 0).astype(F32)[:, None]
 
-    partner = lax.ppermute(gathered, "c", [(0, 1), (1, 0)])
-    top, acc = call(
-        lambda *refs: past_kernel(False, *refs), state, z.reshape(1), gathered, query, top, acc, smem=1
-    )
-    attended, _, _ = call(
-        lambda *refs: past_kernel(True, *refs),
-        (shape((HDIM, tokens)), *state),
-        (z + c).reshape(1),
-        partner,
-        query,
-        top,
-        acc,
-        smem=1,
-    )
-    heads = exchange(jnp.broadcast_to(attended[None], (16, HDIM, tokens)), tp)
+    prepared = (up_weight, targets, out_rows, residual, gain)
+
+    up = down = block
+    top, acc = call(own_kernel, state, c.reshape(1), block, query, smem=1)
+    before = now = (top, acc)
+    chip = z.reshape(1)
+    for k in range(1, chips // 2 + 1):
+        if k == 4:
+            up, down, before, prepared = lax.optimization_barrier((up, down, before, prepared))
+        elif k > 1:
+            up, down, before = lax.optimization_barrier((up, down, before))
+        up = lax.ppermute(up, "z", ahead)
+        arrived, outs = [up], state
+        if k < chips // 2:
+            down = lax.ppermute(down, "z", back)
+            arrived.append(down)
+        else:
+            outs = (*state, shape((80, tokens), F32))
+        kernel = functools.partial(past_kernel, k, chips, len(arrived))
+        before = now
+        now = call(kernel, outs, chip, *arrived, query, *now, smem=1, flops=2**30)
+    top, acc, sent = now
+    up_weight, targets, out_rows, residual, gain = prepared
+    other = lax.ppermute(sent, "c", ((0, 1), (1, 0)))
+    heads = call(merge_kernel, shape((16, HDIM, tokens)), top, acc, other)
+    heads = exchange(heads, tp)
+
     mid, squares = call(
         mid_kernel,
         (shape((128, tokens)), shape((16, 1, tokens), F32)),
         heads.reshape(16 * HDIM, tokens),
-        out_weight.T,
-        residual.T,
+        out_rows,
+        residual,
     )
     squares = exchange(squares, tp)
     rows, normed = call(

time: 344 us -> 293 us (0.85)
  waiting for transfers between devices: 136 us -> 9.02 us
  blocking collectives: 89 us -> 155 us
  starting transfers between devices: 59.3 us -> 79 us
  between operations: 13.5 us -> 0.46 us
  Pallas kernels: 27.1 us -> 39.1 us
  local copies, waits for them, and re-layouts: 13.8 us -> 4.66 us
    all_gather x1 -> x0, waiting for transfers between devices: 69.2 us -> none  [shards(): gathered = lax.all_gather(block, 'z', axis=0, tiled=False)]
    all_to_all x3 -> x5, blocking collectives: 89 us -> 155 us  [exchange(): return lax.all_to_all(array, axis, split_axis=0, concat_axis=0, tiled=True)]
    all_to_all x4 -> x2, waiting for transfers between devices: 66.7 us -> 5.68 us  [exchange(): return lax.all_to_all(array, axis, split_axis=0, concat_axis=0, tiled=True)]
    ppermute x1 -> x17, starting transfers between devices: 11.9 us -> 70.6 us  [the longest x7 31.1 us: shards(): down = lax.ppermute(down, 'z', back)]
    all_to_all x4 -> x2, starting transfers between devices: 47.4 us -> 8.46 us  [exchange(): return lax.all_to_all(array, axis, split_axis=0, concat_axis=0, tiled=True)]
    pallas_call x10 -> x17, Pallas kernels: 27.1 us -> 39.1 us  [call(): pl.pallas_call(kernel, out_shape=outs, in_specs=specs, out_specs=jax.tree...]
    concatenate x1, local copies, waits for them, and re-layouts: 3.56 us -> 0.04 us  [shards(): jnp.concatenate([key_vectors.T, pieces(-gates), ones, zeros, value_vector...]
  transfers between devices with their start and end apart: 6 -> 19, of which waited for: 5 -> 6; matrix products, arithmetic and copies ran while one was open for 2% -> 1% of each run, Pallas kernels for 3% -> 6%
where the time goes in v2:
time: 293 us; the launch traced here: 292 us
  blocking collectives  155 us (53%)
  starting transfers between devices  79 us (27%)
  Pallas kernels  39.1 us (13%)
  waiting for transfers between devices  9.02 us (3%)
  local copies, waits for them, and re-layouts  4.66 us (2%)
  other arithmetic  4.42 us (2%)
    all_to_all x5, blocking collectives, exchange(): return lax.all_to_all(array, axis, split_axis=0, concat_axis=0, tiled=True)  155 us
    pallas_call x17, Pallas kernels, call(): pl.pallas_call(kernel, out_shape=outs, in_specs=specs, out_specs=jax.tree...  39.1 us
    ppermute x7, starting transfers between devices, shards(): down = lax.ppermute(down, 'z', back)  31.1 us
    ppermute x8, starting transfers between devices, shards(): up = lax.ppermute(up, 'z', ahead)  21.9 us
    ppermute x1, starting transfers between devices, shards(): other = lax.ppermute(sent, 'c', ((0, 1), (1, 0)))  10.1 us
    all_to_all x2, starting transfers between devices, exchange(): return lax.all_to_all(array, axis, split_axis=0, concat_axis=0, tiled=True)  8.46 us
    ppermute x1, starting transfers between devices, shards(): lax.ppermute(query, 'c', ((0, 1), (1, 0)))  7.54 us
  transfers between devices with their start and end apart: 19, of which 6 were waited for; matrix products, arithmetic and copies ran while one was open for 1% of the time, Pallas kernels for 6%

profile of v2, /device:TPU:1, one launch (start us, length us, event | category | flops | bytes accessed | tf_op | source)
XLA Modules:
  0.0 291.7 jit_solution(6042599973186513575)
XLA Ops:
  0.0 1.3 maximum_bitcast_fusion
  1.6 1.6 pad_maximum_fusion
  3.2 5.0 %all-to-all-start = ((bf16[4,128,2048]{2,1,0:T(8,128)(2,1)}), bf16[4,128,2048]{2,1,0:T(8,128)(2,1)S(1)}, u32[]{:S(2)}, u32[]{:S(2)}) async-start(bf16[4,128,2048]{2,1,0:T(8,128)(2,1)} %pad_maximum_fusion), calls=%async_computation | async-start | bytes 4194304 | tf_op jit(solution)/shard_map/all_to_all | solution.py:246
  8.3 7.5 %collective-permute-start.2 = (bf16[72,512]{1,0:T(8,128)(2,1)S(1)}, bf16[72,512]{1,0:T(8,128)(2,1)S(1)}, u32[]{:S(2)}, u32[]{:S(2)}) collective-permute-start(bf16[72,512]{1,0:T(8,128)(2,1)S(1)} %concatenate.22), channel_id=1, source_target_pairs={{0,16},{16,0},{1,17},{17,1},{2,18},{18,2},{3,19},{19,3},{4,20},{20... | collective-permute-start | bytes 221192 | tf_op jit(solution)/shard_map/ppermute | solution.py:277
  15.9 6.4 %collective-permute-start.1 = (bf16[136,512]{1,0:T(8,128)(2,1)S(1)}, bf16[136,512]{1,0:T(8,128)(2,1)S(1)}, u32[]{:S(2)}, u32[]{:S(2)}) collective-permute-start(bf16[136,512]{1,0:T(8,128)(2,1)S(1)} %concatenate.21.block_ref), channel_id=1, source_target_pairs={{0,480},{32,0},{64,32},{96,64},{128,96},{160,128},{192,160},{224,1... | collective-permute-start | bytes 417800 | tf_op jit(solution)/shard_map/ppermute | solution.py:306
  22.4 1.3 collective-permute-start
  24.4 2.3 shard_map.145
  26.7 4.1 %collective-permute-start.3 = (bf16[136,512]{1,0:T(8,128)(2,1)S(1)}, bf16[136,512]{1,0:T(8,128)(2,1)S(1)}, u32[]{:S(2)}, u32[]{:S(2)}) collective-permute-start(bf16[136,512]{1,0:T(8,128)(2,1)S(1)} %collective-permute-done.refs_0_), channel_id=1, source_target_pairs={{0,32},{32,64},{64,96},{96,128},{128,160},{160,192},{192,224},{224... | collective-permute-start | bytes 417800 | tf_op jit(solution)/shard_map/ppermute | solution.py:303
  30.8 2.4 collective-permute-start.4
  33.2 2.0 shard_map.146
  35.1 1.4 collective-permute-done.4.refs_1_
  36.6 2.5 collective-permute-start.5
  39.1 3.3 %collective-permute-start.6 = (bf16[136,512]{1,0:T(8,128)(2,1)S(1)}, bf16[136,512]{1,0:T(8,128)(2,1)S(1)}, u32[]{:S(2)}, u32[]{:S(2)}) collective-permute-start(bf16[136,512]{1,0:T(8,128)(2,1)S(1)} %collective-permute-done.4.refs_1_), channel_id=1, source_target_pairs={{0,480},{32,0},{64,32},{96,64},{128,96},{160,128},{192,160},{224,1... | collective-permute-start | bytes 417800 | tf_op jit(solution)/shard_map/ppermute | solution.py:306
  43.1 0.8 copy.18
  43.9 0.8 copy.17
  44.7 1.6 shard_map.148.refs_3_.targets_ref
  46.3 1.9 shard_map.147
  48.3 2.0 collective-permute-start.7
  50.3 5.2 %collective-permute-start.8 = (bf16[136,512]{1,0:T(8,128)(2,1)S(1)}, bf16[136,512]{1,0:T(8,128)(2,1)S(1)}, u32[]{:S(2)}, u32[]{:S(2)}) collective-permute-start(bf16[136,512]{1,0:T(8,128)(2,1)S(1)} %collective-permute-done.6.refs_1_), channel_id=1, source_target_pairs={{0,480},{32,0},{64,32},{96,64},{128,96},{160,128},{192,160},{224,1... | collective-permute-start | bytes 417800 | tf_op jit(solution)/shard_map/ppermute | solution.py:306
  55.6 1.9 shard_map.149
  57.5 1.5 collective-permute-start.9
  59.1 5.6 %collective-permute-start.10 = (bf16[136,512]{1,0:T(8,128)(2,1)S(1)}, bf16[136,512]{1,0:T(8,128)(2,1)S(1)}, u32[]{:S(2)}, u32[]{:S(2)}) collective-permute-start(bf16[136,512]{1,0:T(8,128)(2,1)S(1)} %collective-permute-done.8.refs_1_), channel_id=1, source_target_pairs={{0,480},{32,0},{64,32},{96,64},{128,96},{160,128},{192,160},{224,1... | collective-permute-start | bytes 417800 | tf_op jit(solution)/shard_map/ppermute | solution.py:306
  64.7 1.9 shard_map.150
  66.7 2.5 collective-permute-start.11
  69.2 4.7 %collective-permute-start.12 = (bf16[136,512]{1,0:T(8,128)(2,1)S(1)}, bf16[136,512]{1,0:T(8,128)(2,1)S(1)}, u32[]{:S(2)}, u32[]{:S(2)}) collective-permute-start(bf16[136,512]{1,0:T(8,128)(2,1)S(1)} %collective-permute-done.10.refs_1_), channel_id=1, source_target_pairs={{0,480},{32,0},{64,32},{96,64},{128,96},{160,128},{192,160},{224,1... | collective-permute-start | bytes 417800 | tf_op jit(solution)/shard_map/ppermute | solution.py:306
  73.9 1.9 shard_map.151
  75.9 4.5 %collective-permute-start.13 = (bf16[136,512]{1,0:T(8,128)(2,1)S(1)}, bf16[136,512]{1,0:T(8,128)(2,1)S(1)}, u32[]{:S(2)}, u32[]{:S(2)}) collective-permute-start(bf16[136,512]{1,0:T(8,128)(2,1)S(1)} %collective-permute-done.11.refs_0_), channel_id=1, source_target_pairs={{0,32},{32,64},{64,96},{96,128},{128,160},{160,192},{192,224},{224... | collective-permute-start | bytes 417800 | tf_op jit(solution)/shard_map/ppermute | solution.py:303
  80.4 3.4 %collective-permute-start.14 = (bf16[136,512]{1,0:T(8,128)(2,1)S(1)}, bf16[136,512]{1,0:T(8,128)(2,1)S(1)}, u32[]{:S(2)}, u32[]{:S(2)}) collective-permute-start(bf16[136,512]{1,0:T(8,128)(2,1)S(1)} %collective-permute-done.12.refs_1_), channel_id=1, source_target_pairs={{0,480},{32,0},{64,32},{96,64},{128,96},{160,128},{192,160},{224,1... | collective-permute-start | bytes 417800 | tf_op jit(solution)/shard_map/ppermute | solution.py:306
  83.9 1.9 shard_map.152
  86.3 3.5 %collective-permute-start.15 = (bf16[136,512]{1,0:T(8,128)(2,1)S(1)}, bf16[136,512]{1,0:T(8,128)(2,1)S(1)}, u32[]{:S(2)}, u32[]{:S(2)}) collective-permute-start(bf16[136,512]{1,0:T(8,128)(2,1)S(1)} %collective-permute-done.13.refs_0_), channel_id=1, source_target_pairs={{0,32},{32,64},{64,96},{96,128},{128,160},{160,192},{192,224},{224... | collective-permute-start | bytes 417800 | tf_op jit(solution)/shard_map/ppermute | solution.py:303
  89.9 1.9 shard_map.153
  92.5 1.9 shard_map.154
  94.4 10.1 %collective-permute-start.16 = (f32[80,512]{1,0:T(8,128)}, f32[80,512]{1,0:T(8,128)S(1)}, u32[]{:S(2)}, u32[]{:S(2)}) collective-permute-start(f32[80,512]{1,0:T(8,128)} %get-tuple-element.79), channel_id=1, source_target_pairs={{0,16},{16,0},{1,17},{17,1},{2,18},{18,2},{3,19},{19,3},{4,20},{20... | collective-permute-start | bytes 491528 | tf_op jit(solution)/shard_map/ppermute | solution.py:315
  104.5 1.2 collective-permute-done.16.other_ref
  106.4 2.1 shard_map.155
  108.5 23.7 %all_to_all.35 = bf16[16,64,512]{2,1,0:T(8,128)(2,1)} all-to-all(bf16[16,64,512]{2,1,0:T(8,128)(2,1)} %shard_map.155), channel_id=1, replica_groups=mesh['z'=16,'c'=2,'y'=4,'x'=4] {'y','x'}, dimensions={0} | all-to-all | bytes 2097152 | tf_op jit(solution)/shard_map/all_to_all | solution.py:246
  132.2 2.3 shard_map.156
  134.6 3.5 %all-to-all-start.2 = ((f32[16,1,512]{2,1,0:T(1,128)}), f32[16,1,512]{2,1,0:T(1,128)S(1)}, u32[]{:S(2)}, u32[]{:S(2)}) async-start(f32[16,1,512]{2,1,0:T(1,128)} %get-tuple-element.83), calls=%async_computation.2 | async-start | bytes 65536 | tf_op jit(solution)/shard_map/all_to_all | solution.py:246
  138.8 5.7 %all-to-all-done.2.refs_1_ = f32[16,1,512]{2,1,0:T(1,128)S(1)} async-done(((f32[16,1,512]{2,1,0:T(1,128)}), f32[16,1,512]{2,1,0:T(1,128)S(1)}, u32[]{:S(2)}, u32[]{:S(2)}) %all-to-all-start.2) | async-done | bytes 32800 | tf_op jit(solution)/shard_map/all_to_all | solution.py:246
  145.1 2.4 shard_map.157
  147.5 41.6 %all_to_all.36 = bf16[32,40,128]{2,1,0:T(8,128)(2,1)} all-to-all(bf16[32,40,128]{2,1,0:T(8,128)(2,1)} %bitcast.49), channel_id=1, replica_groups=mesh['z'=16,'c'=2,'y'=4,'x'=4] {'z','c'}, dimensions={0} | all-to-all | bytes 655360 | tf_op jit(solution)/shard_map/all_to_all | solution.py:246
  189.1 2.7 shard_map.158
  191.8 29.4 %all_to_all.37.rows_ref = bf16[16,448,128]{2,1,0:T(8,128)(2,1)} all-to-all(bf16[16,448,128]{2,1,0:T(8,128)(2,1)} %shard_map.158), channel_id=1, replica_groups=mesh['z'=16,'c'=2,'y'=4,'x'=4] {'y','x'}, dimensions={0} | all-to-all | bytes 3670016 | tf_op jit(solution)/shard_map/all_to_all | solution.py:246
  221.3 4.4 %shard_map.159 = bf16[16,448,128]{2,1,0:T(8,128)(2,1)} custom-call(bf16[16,448,128]{2,1,0:T(8,128)(2,1)} %all_to_all.37.rows_ref, bf16[4,128,2048]{2,1,0:T(8,128)(2,1)} %copy-done), custom_call_target="tpu_custom_call" | custom-call | flops 268435456 | bytes 4194304 | tf_op jit(solution)/shard_map/pallas_call | solution.py:27
  225.6 28.5 %all_to_all.38.hidden_ref = bf16[16,448,128]{2,1,0:T(8,128)(2,1)} all-to-all(bf16[16,448,128]{2,1,0:T(8,128)(2,1)} %shard_map.159), channel_id=1, replica_groups=mesh['z'=16,'c'=2,'y'=4,'x'=4] {'y','x'}, dimensions={0} | all-to-all | bytes 3670016 | tf_op jit(solution)/shard_map/all_to_all | solution.py:246
  254.1 3.4 %shard_map.160 = (bf16[1280,128]{1,0:T(8,128)(2,1)}, f32[512,128]{1,0:T(8,128)}) custom-call(bf16[16,448,128]{2,1,0:T(8,128)(2,1)} %all_to_all.38.hidden_ref, bf16[4,512,128]{2,1,0:T(8,128)(2,1)} %weight_ref.1, bf16[512,128]{1,0:T(8,128)(2,1)} %shared_ref.1), custom_call_target="tpu_custom_call" | custom-call | flops 268435456 | bytes 4194304 | tf_op jit(solution)/shard_map/pallas_call | solution.py:27
  257.5 31.7 %all_to_all.39 = bf16[32,40,128]{2,1,0:T(8,128)(2,1)} all-to-all(bf16[32,40,128]{2,1,0:T(8,128)(2,1)} %bitcast.50), channel_id=1, replica_groups=mesh['z'=16,'c'=2,'y'=4,'x'=4] {'z','c'}, dimensions={0} | all-to-all | bytes 655360 | tf_op jit(solution)/shard_map/all_to_all | solution.py:246
  289.2 2.5 shard_map.161
  (82 shorter events, 5.2 us)
Async XLA Ops:
  0.0 1.4 copy-start.5
  0.0 1.4 copy-start.6
  3.2 5.0 %copy-start.11 = (f32[512,1]{0,1:T(1,128)S(1)}, f32[512,1]{0,1:T(1,128)}, u32[]{:S(2)}) copy-start(f32[512,1]{0,1:T(1,128)} %param.18) | copy-start | bytes 6148
  3.2 5.0 %copy-start.9 = (bf16[512,64]{0,1:T(8,128)(2,1)S(1)}, bf16[512,64]{0,1:T(8,128)(2,1)}, u32[]{:S(2)}) copy-start(bf16[512,64]{0,1:T(8,128)(2,1)} %param.15) | copy-start | bytes 196612
  3.2 12.6 %copy-start.7 = (bf16[512,64]{0,1:T(8,128)(2,1)S(1)}, bf16[512,64]{0,1:T(8,128)(2,1)}, u32[]{:S(2)}) copy-start(bf16[512,64]{0,1:T(8,128)(2,1)} %param.16) | copy-start | bytes 196612
  3.2 12.6 %copy-start.8 = (bf16[512,64]{0,1:T(8,128)(2,1)S(1)}, bf16[512,64]{0,1:T(8,128)(2,1)}, u32[]{:S(2)}) copy-start(bf16[512,64]{0,1:T(8,128)(2,1)} %param.17) | copy-start | bytes 196612
  3.2 45.1 %all-to-all-start = ((bf16[4,128,2048]{2,1,0:T(8,128)(2,1)}), bf16[4,128,2048]{2,1,0:T(8,128)(2,1)S(1)}, u32[]{:S(2)}, u32[]{:S(2)}) async-start(bf16[4,128,2048]{2,1,0:T(8,128)(2,1)} %pad_maximum_fusion), calls=%async_computation | async-start | bytes 4194304 | tf_op jit(solution)/shard_map/all_to_all | solution.py:246
  8.3 15.4 %collective-permute-start.2 = (bf16[72,512]{1,0:T(8,128)(2,1)S(1)}, bf16[72,512]{1,0:T(8,128)(2,1)S(1)}, u32[]{:S(2)}, u32[]{:S(2)}) collective-permute-start(bf16[72,512]{1,0:T(8,128)(2,1)S(1)} %concatenate.22), channel_id=1, source_target_pairs={{0,16},{16,0},{1,17},{17,1},{2,18},{18,2},{3,19},{19,3},{4,20},{20... | collective-permute-start | bytes 221192 | tf_op jit(solution)/shard_map/ppermute | solution.py:277
  15.9 8.5 %copy-start.3 = (bf16[136,512]{1,0:T(8,128)(2,1)}, bf16[136,512]{1,0:T(8,128)(2,1)S(1)}, u32[]{:S(2)}) copy-start(bf16[136,512]{1,0:T(8,128)(2,1)S(1)} %concatenate.21.block_ref) | copy-start | bytes 417796
  15.9 10.7 %collective-permute-start.1 = (bf16[136,512]{1,0:T(8,128)(2,1)S(1)}, bf16[136,512]{1,0:T(8,128)(2,1)S(1)}, u32[]{:S(2)}, u32[]{:S(2)}) collective-permute-start(bf16[136,512]{1,0:T(8,128)(2,1)S(1)} %concatenate.21.block_ref), channel_id=1, source_target_pairs={{0,480},{32,0},{64,32},{96,64},{128,96},{160,128},{192,160},{224,1... | collective-permute-start | bytes 417800 | tf_op jit(solution)/shard_map/ppermute | solution.py:306
  22.4 4.3 %collective-permute-start = (bf16[136,512]{1,0:T(8,128)(2,1)S(1)}, bf16[136,512]{1,0:T(8,128)(2,1)S(1)}, u32[]{:S(2)}, u32[]{:S(2)}) collective-permute-start(bf16[136,512]{1,0:T(8,128)(2,1)S(1)} %concatenate.21.block_ref), channel_id=1, source_target_pairs={{0,32},{32,64},{64,96},{96,128},{128,160},{160,192},{192,224},{224... | collective-permute-start | bytes 417800 | tf_op jit(solution)/shard_map/ppermute | solution.py:303
  26.6 16.5 %copy-start.4 = (bf16[512,128]{1,0:T(8,128)(2,1)S(1)}, bf16[512,128]{1,0:T(8,128)(2,1)}, u32[]{:S(2)}) copy-start(bf16[512,128]{1,0:T(8,128)(2,1)} %param.19) | copy-start | bytes 393220
  26.7 6.5 %copy-start.12 = (bf16[136,512]{1,0:T(8,128)(2,1)}, bf16[136,512]{1,0:T(8,128)(2,1)S(1)}, u32[]{:S(2)}) copy-start(bf16[136,512]{1,0:T(8,128)(2,1)S(1)} %collective-permute-done.1.refs_1_) | copy-start | bytes 417796
  26.7 6.5 %copy-start.13 = (bf16[136,512]{1,0:T(8,128)(2,1)}, bf16[136,512]{1,0:T(8,128)(2,1)S(1)}, u32[]{:S(2)}) copy-start(bf16[136,512]{1,0:T(8,128)(2,1)S(1)} %collective-permute-done.refs_0_) | copy-start | bytes 417796
  26.7 8.5 %collective-permute-start.3 = (bf16[136,512]{1,0:T(8,128)(2,1)S(1)}, bf16[136,512]{1,0:T(8,128)(2,1)S(1)}, u32[]{:S(2)}, u32[]{:S(2)}) collective-permute-start(bf16[136,512]{1,0:T(8,128)(2,1)S(1)} %collective-permute-done.refs_0_), channel_id=1, source_target_pairs={{0,32},{32,64},{64,96},{96,128},{128,160},{160,192},{192,224},{224... | collective-permute-start | bytes 417800 | tf_op jit(solution)/shard_map/ppermute | solution.py:303
  30.8 5.8 %collective-permute-start.4 = (bf16[136,512]{1,0:T(8,128)(2,1)S(1)}, bf16[136,512]{1,0:T(8,128)(2,1)S(1)}, u32[]{:S(2)}, u32[]{:S(2)}) collective-permute-start(bf16[136,512]{1,0:T(8,128)(2,1)S(1)} %collective-permute-done.1.refs_1_), channel_id=1, source_target_pairs={{0,480},{32,0},{64,32},{96,64},{128,96},{160,128},{192,160},{224,1... | collective-permute-start | bytes 417800 | tf_op jit(solution)/shard_map/ppermute | solution.py:306
  33.2 10.7 %copy-start.1 = (bf16[1024,128]{1,0:T(8,128)(2,1)S(1)}, bf16[1024,128]{1,0:T(8,128)(2,1)}, u32[]{:S(2)}) copy-start(bf16[1024,128]{1,0:T(8,128)(2,1)} %param.20) | copy-start | bytes 786436
  35.1 11.2 %copy-start.14 = (bf16[136,512]{1,0:T(8,128)(2,1)}, bf16[136,512]{1,0:T(8,128)(2,1)S(1)}, u32[]{:S(2)}) copy-start(bf16[136,512]{1,0:T(8,128)(2,1)S(1)} %collective-permute-done.3.refs_0_) | copy-start | bytes 417796
  36.6 9.8 %copy-start.15 = (bf16[136,512]{1,0:T(8,128)(2,1)}, bf16[136,512]{1,0:T(8,128)(2,1)S(1)}, u32[]{:S(2)}) copy-start(bf16[136,512]{1,0:T(8,128)(2,1)S(1)} %collective-permute-done.4.refs_1_) | copy-start | bytes 417796
  36.6 11.7 %collective-permute-start.5 = (bf16[136,512]{1,0:T(8,128)(2,1)S(1)}, bf16[136,512]{1,0:T(8,128)(2,1)S(1)}, u32[]{:S(2)}, u32[]{:S(2)}) collective-permute-start(bf16[136,512]{1,0:T(8,128)(2,1)S(1)} %collective-permute-done.3.refs_0_), channel_id=1, source_target_pairs={{0,32},{32,64},{64,96},{96,128},{128,160},{160,192},{192,224},{224... | collective-permute-start | bytes 417800 | tf_op jit(solution)/shard_map/ppermute | solution.py:303
  39.1 9.2 %collective-permute-start.6 = (bf16[136,512]{1,0:T(8,128)(2,1)S(1)}, bf16[136,512]{1,0:T(8,128)(2,1)S(1)}, u32[]{:S(2)}, u32[]{:S(2)}) collective-permute-start(bf16[136,512]{1,0:T(8,128)(2,1)S(1)} %collective-permute-done.4.refs_1_), channel_id=1, source_target_pairs={{0,480},{32,0},{64,32},{96,64},{128,96},{160,128},{192,160},{224,1... | collective-permute-start | bytes 417800 | tf_op jit(solution)/shard_map/ppermute | solution.py:306
  48.3 7.2 %copy-start.16 = (bf16[136,512]{1,0:T(8,128)(2,1)}, bf16[136,512]{1,0:T(8,128)(2,1)S(1)}, u32[]{:S(2)}) copy-start(bf16[136,512]{1,0:T(8,128)(2,1)S(1)} %collective-permute-done.5.refs_0_) | copy-start | bytes 417796
  48.3 7.2 %copy-start.17 = (bf16[136,512]{1,0:T(8,128)(2,1)}, bf16[136,512]{1,0:T(8,128)(2,1)S(1)}, u32[]{:S(2)}) copy-start(bf16[136,512]{1,0:T(8,128)(2,1)S(1)} %collective-permute-done.6.refs_1_) | copy-start | bytes 417796
  48.3 18.3 %copy-start = (bf16[4,128,2048]{2,1,0:T(8,128)(2,1)}, bf16[4,128,2048]{2,1,0:T(8,128)(2,1)S(1)}, u32[]{:S(2)}) copy-start(bf16[4,128,2048]{2,1,0:T(8,128)(2,1)S(1)} %all-to-all-done.weight_ref) | copy-start | bytes 6291460
  48.3 9.1 %collective-permute-start.7 = (bf16[136,512]{1,0:T(8,128)(2,1)S(1)}, bf16[136,512]{1,0:T(8,128)(2,1)S(1)}, u32[]{:S(2)}, u32[]{:S(2)}) collective-permute-start(bf16[136,512]{1,0:T(8,128)(2,1)S(1)} %collective-permute-done.5.refs_0_), channel_id=1, source_target_pairs={{0,32},{32,64},{64,96},{96,128},{128,160},{160,192},{192,224},{224... | collective-permute-start | bytes 417800 | tf_op jit(solution)/shard_map/ppermute | solution.py:303
  50.3 7.2 %collective-permute-start.8 = (bf16[136,512]{1,0:T(8,128)(2,1)S(1)}, bf16[136,512]{1,0:T(8,128)(2,1)S(1)}, u32[]{:S(2)}, u32[]{:S(2)}) collective-permute-start(bf16[136,512]{1,0:T(8,128)(2,1)S(1)} %collective-permute-done.6.refs_1_), channel_id=1, source_target_pairs={{0,480},{32,0},{64,32},{96,64},{128,96},{160,128},{192,160},{224,1... | collective-permute-start | bytes 417800 | tf_op jit(solution)/shard_map/ppermute | solution.py:306
  57.5 7.2 %copy-start.18 = (bf16[136,512]{1,0:T(8,128)(2,1)}, bf16[136,512]{1,0:T(8,128)(2,1)S(1)}, u32[]{:S(2)}) copy-start(bf16[136,512]{1,0:T(8,128)(2,1)S(1)} %collective-permute-done.7.refs_0_) | copy-start | bytes 417796
  57.5 7.2 %copy-start.19 = (bf16[136,512]{1,0:T(8,128)(2,1)}, bf16[136,512]{1,0:T(8,128)(2,1)S(1)}, u32[]{:S(2)}) copy-start(bf16[136,512]{1,0:T(8,128)(2,1)S(1)} %collective-permute-done.8.refs_1_) | copy-start | bytes 417796
  57.5 9.1 %collective-permute-start.9 = (bf16[136,512]{1,0:T(8,128)(2,1)S(1)}, bf16[136,512]{1,0:T(8,128)(2,1)S(1)}, u32[]{:S(2)}, u32[]{:S(2)}) collective-permute-start(bf16[136,512]{1,0:T(8,128)(2,1)S(1)} %collective-permute-done.7.refs_0_), channel_id=1, source_target_pairs={{0,32},{32,64},{64,96},{96,128},{128,160},{160,192},{192,224},{224... | collective-permute-start | bytes 417800 | tf_op jit(solution)/shard_map/ppermute | solution.py:303
  59.1 7.6 %collective-permute-start.10 = (bf16[136,512]{1,0:T(8,128)(2,1)S(1)}, bf16[136,512]{1,0:T(8,128)(2,1)S(1)}, u32[]{:S(2)}, u32[]{:S(2)}) collective-permute-start(bf16[136,512]{1,0:T(8,128)(2,1)S(1)} %collective-permute-done.8.refs_1_), channel_id=1, source_target_pairs={{0,480},{32,0},{64,32},{96,64},{128,96},{160,128},{192,160},{224,1... | collective-permute-start | bytes 417800 | tf_op jit(solution)/shard_map/ppermute | solution.py:306
  66.7 7.2 %copy-start.20 = (bf16[136,512]{1,0:T(8,128)(2,1)}, bf16[136,512]{1,0:T(8,128)(2,1)S(1)}, u32[]{:S(2)}) copy-start(bf16[136,512]{1,0:T(8,128)(2,1)S(1)} %collective-permute-done.9.refs_0_) | copy-start | bytes 417796
  66.7 7.2 %copy-start.21 = (bf16[136,512]{1,0:T(8,128)(2,1)}, bf16[136,512]{1,0:T(8,128)(2,1)S(1)}, u32[]{:S(2)}) copy-start(bf16[136,512]{1,0:T(8,128)(2,1)S(1)} %collective-permute-done.10.refs_1_) | copy-start | bytes 417796
  66.7 9.1 %collective-permute-start.11 = (bf16[136,512]{1,0:T(8,128)(2,1)S(1)}, bf16[136,512]{1,0:T(8,128)(2,1)S(1)}, u32[]{:S(2)}, u32[]{:S(2)}) collective-permute-start(bf16[136,512]{1,0:T(8,128)(2,1)S(1)} %collective-permute-done.9.refs_0_), channel_id=1, source_target_pairs={{0,32},{32,64},{64,96},{96,128},{128,160},{160,192},{192,224},{224... | collective-permute-start | bytes 417800 | tf_op jit(solution)/shard_map/ppermute | solution.py:303
  69.2 6.7 %collective-permute-start.12 = (bf16[136,512]{1,0:T(8,128)(2,1)S(1)}, bf16[136,512]{1,0:T(8,128)(2,1)S(1)}, u32[]{:S(2)}, u32[]{:S(2)}) collective-permute-start(bf16[136,512]{1,0:T(8,128)(2,1)S(1)} %collective-permute-done.10.refs_1_), channel_id=1, source_target_pairs={{0,480},{32,0},{64,32},{96,64},{128,96},{160,128},{192,160},{224,1... | collective-permute-start | bytes 417800 | tf_op jit(solution)/shard_map/ppermute | solution.py:306
  75.8 8.0 %copy-start.22 = (bf16[136,512]{1,0:T(8,128)(2,1)}, bf16[136,512]{1,0:T(8,128)(2,1)S(1)}, u32[]{:S(2)}) copy-start(bf16[136,512]{1,0:T(8,128)(2,1)S(1)} %collective-permute-done.11.refs_0_) | copy-start | bytes 417796
  75.9 8.0 %copy-start.23 = (bf16[136,512]{1,0:T(8,128)(2,1)}, bf16[136,512]{1,0:T(8,128)(2,1)S(1)}, u32[]{:S(2)}) copy-start(bf16[136,512]{1,0:T(8,128)(2,1)S(1)} %collective-permute-done.12.refs_1_) | copy-start | bytes 417796
  75.9 9.9 %collective-permute-start.13 = (bf16[136,512]{1,0:T(8,128)(2,1)S(1)}, bf16[136,512]{1,0:T(8,128)(2,1)S(1)}, u32[]{:S(2)}, u32[]{:S(2)}) collective-permute-start(bf16[136,512]{1,0:T(8,128)(2,1)S(1)} %collective-permute-done.11.refs_0_), channel_id=1, source_target_pairs={{0,32},{32,64},{64,96},{96,128},{128,160},{160,192},{192,224},{224... | collective-permute-start | bytes 417800 | tf_op jit(solution)/shard_map/ppermute | solution.py:303
  80.4 5.9 %collective-permute-start.14 = (bf16[136,512]{1,0:T(8,128)(2,1)S(1)}, bf16[136,512]{1,0:T(8,128)(2,1)S(1)}, u32[]{:S(2)}, u32[]{:S(2)}) collective-permute-start(bf16[136,512]{1,0:T(8,128)(2,1)S(1)} %collective-permute-done.12.refs_1_), channel_id=1, source_target_pairs={{0,480},{32,0},{64,32},{96,64},{128,96},{160,128},{192,160},{224,1... | collective-permute-start | bytes 417800 | tf_op jit(solution)/shard_map/ppermute | solution.py:306
  85.8 4.1 %copy-start.24 = (bf16[136,512]{1,0:T(8,128)(2,1)}, bf16[136,512]{1,0:T(8,128)(2,1)S(1)}, u32[]{:S(2)}) copy-start(bf16[136,512]{1,0:T(8,128)(2,1)S(1)} %collective-permute-done.13.refs_0_) | copy-start | bytes 417796
  86.3 3.6 %copy-start.25 = (bf16[136,512]{1,0:T(8,128)(2,1)}, bf16[136,512]{1,0:T(8,128)(2,1)S(1)}, u32[]{:S(2)}) copy-start(bf16[136,512]{1,0:T(8,128)(2,1)S(1)} %collective-permute-done.14.refs_1_) | copy-start | bytes 417796
  86.3 5.5 %collective-permute-start.15 = (bf16[136,512]{1,0:T(8,128)(2,1)S(1)}, bf16[136,512]{1,0:T(8,128)(2,1)S(1)}, u32[]{:S(2)}, u32[]{:S(2)}) collective-permute-start(bf16[136,512]{1,0:T(8,128)(2,1)S(1)} %collective-permute-done.13.refs_0_), channel_id=1, source_target_pairs={{0,32},{32,64},{64,96},{96,128},{128,160},{160,192},{192,224},{224... | collective-permute-start | bytes 417800 | tf_op jit(solution)/shard_map/ppermute | solution.py:303
  91.8 0.7 copy-start.26
  94.4 11.4 %collective-permute-start.16 = (f32[80,512]{1,0:T(8,128)}, f32[80,512]{1,0:T(8,128)S(1)}, u32[]{:S(2)}, u32[]{:S(2)}) collective-permute-start(f32[80,512]{1,0:T(8,128)} %get-tuple-element.79), channel_id=1, source_target_pairs={{0,16},{16,0},{1,17},{17,1},{2,18},{18,2},{3,19},{19,3},{4,20},{20... | collective-permute-start | bytes 491528 | tf_op jit(solution)/shard_map/ppermute | solution.py:315
  105.8 0.7 copy-start.2
  134.6 9.9 %all-to-all-start.2 = ((f32[16,1,512]{2,1,0:T(1,128)}), f32[16,1,512]{2,1,0:T(1,128)S(1)}, u32[]{:S(2)}, u32[]{:S(2)}) async-start(f32[16,1,512]{2,1,0:T(1,128)} %get-tuple-element.83), calls=%async_computation.2 | async-start | bytes 65536 | tf_op jit(solution)/shard_map/all_to_all | solution.py:246
  144.5 0.6 copy-start.10

commit v3 on v2

--- a/solution.py
+++ b/solution.py
@@ -6,6 +6,7 @@
 from jax.experimental import pallas as pl
 from jax.experimental.pallas import tpu as pltpu
 from jax.sharding import Mesh, PartitionSpec as P
+
 
 HDIM = 64
 EPSILON = 1e-06
@@ -21,7 +22,7 @@
     return lax.dot_general(a, b, dims, preferred_element_type=F32)
 
 
-def call(kernel, outs, *args, smem=0, scratch=(), flops=2**28, nbytes=2**22):
+def call(kernel, outs, *args, smem=0, scratch=(), flops=2**28, nbytes=2**22, limit=2**24):
     specs = [pl.BlockSpec(memory_space=pltpu.SMEM)] * smem
     specs += [pl.BlockSpec(memory_space=pltpu.VMEM)] * (len(args) - smem)
     return pl.pallas_call(
@@ -30,6 +31,7 @@
         in_specs=specs,
         out_specs=jax.tree.map(lambda _: pl.BlockSpec(memory_space=pltpu.VMEM), outs),
         scratch_shapes=scratch,
+        compiler_params=pltpu.CompilerParams(vmem_limit_bytes=limit),
         cost_estimate=pl.CostEstimate(flops=flops, bytes_accessed=nbytes, transcendentals=0),
     )(*args)
 
@@ -82,7 +84,7 @@
     top_ref[...] = top_in[...]
     acc_ref[...] = acc_in[...]
     chip = chip_ref[0]
-    for useful, block_ref in zip((chip >= k, chip + k >= chips), blocks):
+    for useful, block_ref in zip((chip + k >= chips, chip >= k)[-count:], blocks):
 
         @pl.when(useful)
         def _():
@@ -218,7 +220,6 @@
 
 
 def last_kernel(returned_ref, targets_ref, weight_ref, mid_ref, shared_ref, out_ref):
-    tokens = targets_ref.shape[1]
     total = mid_ref[...].astype(F32)
     slots = returned_ref.shape[0]
     chunk = slots // 5
@@ -277,8 +278,6 @@
     query = jnp.concatenate([query, lax.ppermute(query, "c", ((0, 1), (1, 0)))], axis=1)
     state = (shape((1, 2 * tokens), F32), shape((72, 2 * tokens), F32))
     chips = lax.axis_size("z")
-    ahead = [(i, i + 1) for i in range(chips - 1)]
-    back = [(i, (i - 1) % chips) for i in range(chips)]
 
     local = jnp.stack([expert_gate, expert_up], axis=1).transpose(0, 1, 3, 2).reshape(4, 64, width)
     both = jnp.concatenate([shared_gate.T, shared_up.T], axis=0)
@@ -300,13 +299,15 @@
             up, down, before, prepared = lax.optimization_barrier((up, down, before, prepared))
         elif k > 1:
             up, down, before = lax.optimization_barrier((up, down, before))
-        up = lax.ppermute(up, "z", ahead)
-        arrived, outs = [up], state
+        arrived, outs = [], state
         if k < chips // 2:
+            back = [((i - k + 1) % chips, (i - k) % chips) for i in range(chips // 2 - 1)]
             down = lax.ppermute(down, "z", back)
             arrived.append(down)
         else:
             outs = (*state, shape((80, tokens), F32))
+        up = lax.ppermute(up, "z", [(i, i + 1) for i in range(k - 1, chips - 1)])
+        arrived.append(up)
         kernel = functools.partial(past_kernel, k, chips, len(arrived))
         before = now
         now = call(kernel, outs, chip, *arrived, query, *now, smem=1, flops=2**30)

time: 293 us -> 261 us (0.89)
  Pallas kernels: 39.1 us -> 6.84 us
  waiting for transfers between devices: 9.02 us -> 19.9 us
  starting transfers between devices: 79 us -> 69.9 us
    pallas_call x17, Pallas kernels: 39.1 us -> 6.84 us  [call(): pl.pallas_call(kernel, out_shape=outs, in_specs=specs, out_specs=jax.tree...]
    ppermute x8, starting transfers between devices: 21.9 us -> 5.91 us  [shards(): up = lax.ppermute(up, 'z', [(i, i + 1) for i in range(k - 1, chips - 1)])]
    ppermute x7, waiting for transfers between devices: 2.1 us -> 11.3 us  [shards(): down = lax.ppermute(down, 'z', back)]
    ppermute x7, starting transfers between devices: 31.1 us -> 39.5 us  [shards(): down = lax.ppermute(down, 'z', back)]
  transfers between devices with their start and end apart: 19 -> 19, of which waited for: 6 -> 9; matrix products, arithmetic and copies ran while one was open for 1% -> 1% of each run, Pallas kernels for 6% -> 0%
where the time goes in v3:
time: 261 us; the launch traced here: 260 us
  blocking collectives  156 us (60%)
  starting transfers between devices  69.9 us (27%)
  waiting for transfers between devices  19.9 us (8%)
  Pallas kernels  6.84 us (3%)
  other arithmetic  3.76 us (1%)
  local copies, waits for them, and re-layouts  3.3 us (1%)
    all_to_all x5, blocking collectives, exchange(): return lax.all_to_all(array, axis, split_axis=0, concat_axis=0, tiled=True)  156 us
    ppermute x7, starting transfers between devices, shards(): down = lax.ppermute(down, 'z', back)  39.5 us
    ppermute x7, waiting for transfers between devices, shards(): down = lax.ppermute(down, 'z', back)  11.3 us
    ppermute x1, starting transfers between devices, shards(): other = lax.ppermute(sent, 'c', ((0, 1), (1, 0)))  8.49 us
    all_to_all x2, starting transfers between devices, exchange(): return lax.all_to_all(array, axis, split_axis=0, concat_axis=0, tiled=True)  8.47 us
    ppermute x1, starting transfers between devices, shards(): lax.ppermute(query, 'c', ((0, 1), (1, 0)))  7.54 us
    pallas_call x17, Pallas kernels, call(): pl.pallas_call(kernel, out_shape=outs, in_specs=specs, out_specs=jax.tree...  6.84 us
    all_to_all x2, waiting for transfers between devices, exchange(): return lax.all_to_all(array, axis, split_axis=0, concat_axis=0, tiled=True)  6.29 us
  transfers between devices with their start and end apart: 19, of which 9 were waited for; matrix products, arithmetic and copies ran while one was open for 1% of the time, Pallas kernels for 0%

profile of v3, /device:TPU:1, one launch (start us, length us, event | category | flops | bytes accessed | tf_op | source)
XLA Modules:
  0.0 260.3 jit_solution(7390082311845742168)
XLA Ops:
  0.0 1.3 maximum_bitcast_fusion
  1.6 1.6 pad_maximum_fusion
  3.2 5.0 %all-to-all-start = ((bf16[4,128,2048]{2,1,0:T(8,128)(2,1)}), bf16[4,128,2048]{2,1,0:T(8,128)(2,1)S(1)}, u32[]{:S(2)}, u32[]{:S(2)}) async-start(bf16[4,128,2048]{2,1,0:T(8,128)(2,1)} %pad_maximum_fusion), calls=%async_computation | async-start | bytes 4194304 | tf_op jit(solution)/shard_map/all_to_all | solution.py:247
  8.3 7.5 %collective-permute-start.2 = (bf16[72,512]{1,0:T(8,128)(2,1)S(1)}, bf16[72,512]{1,0:T(8,128)(2,1)S(1)}, u32[]{:S(2)}, u32[]{:S(2)}) collective-permute-start(bf16[72,512]{1,0:T(8,128)(2,1)S(1)} %concatenate.22), channel_id=1, source_target_pairs={{0,16},{16,0},{1,17},{17,1},{2,18},{18,2},{3,19},{19,3},{4,20},{20... | collective-permute-start | bytes 221192 | tf_op jit(solution)/shard_map/ppermute | solution.py:278
  15.9 6.4 %collective-permute-start.1 = (bf16[136,512]{1,0:T(8,128)(2,1)S(1)}, bf16[136,512]{1,0:T(8,128)(2,1)S(1)}, u32[]{:S(2)}, u32[]{:S(2)}) collective-permute-start(bf16[136,512]{1,0:T(8,128)(2,1)S(1)} %concatenate.21.block_ref), channel_id=1, source_target_pairs={{0,480},{32,0},{64,32},{96,64},{128,96},{160,128},{192,160},{1,481... | collective-permute-start | bytes 417800 | tf_op jit(solution)/shard_map/ppermute | solution.py:305
  22.4 1.3 collective-permute-start
  23.7 0.6 shard_map.145
  24.3 1.1 collective-permute-done.1.refs_0_
  25.4 1.3 collective-permute-done.refs_1_
  26.7 0.7 collective-permute-start.3
  27.3 4.7 %collective-permute-start.4 = (bf16[136,512]{1,0:T(8,128)(2,1)S(1)}, bf16[136,512]{1,0:T(8,128)(2,1)S(1)}, u32[]{:S(2)}, u32[]{:S(2)}) collective-permute-start(bf16[136,512]{1,0:T(8,128)(2,1)S(1)} %collective-permute-done.1.refs_0_), channel_id=1, source_target_pairs={{480,448},{0,480},{32,0},{64,32},{96,64},{128,96},{160,128},{481,4... | collective-permute-start | bytes 417800 | tf_op jit(solution)/shard_map/ppermute | solution.py:305
  32.2 0.7 copy-done.4
  32.9 2.4 collective-permute-done.4.refs_0_
  35.2 0.7 collective-permute-start.5
  35.9 4.9 %collective-permute-start.6 = (bf16[136,512]{1,0:T(8,128)(2,1)S(1)}, bf16[136,512]{1,0:T(8,128)(2,1)S(1)}, u32[]{:S(2)}, u32[]{:S(2)}) collective-permute-start(bf16[136,512]{1,0:T(8,128)(2,1)S(1)} %collective-permute-done.4.refs_0_), channel_id=1, source_target_pairs={{448,416},{480,448},{0,480},{32,0},{64,32},{96,64},{128,96},{449,4... | collective-permute-start | bytes 417800 | tf_op jit(solution)/shard_map/ppermute | solution.py:305
  40.8 0.8 bitcast_convert_fusion
  41.6 1.0 copy.18
  42.8 0.3 shard_map.148.refs_3_.targets_ref
  43.1 1.0 copy-done.5
  44.1 0.7 collective-permute-start.7
  44.8 6.5 %collective-permute-start.8 = (bf16[136,512]{1,0:T(8,128)(2,1)S(1)}, bf16[136,512]{1,0:T(8,128)(2,1)S(1)}, u32[]{:S(2)}, u32[]{:S(2)}) collective-permute-start(bf16[136,512]{1,0:T(8,128)(2,1)S(1)} %collective-permute-done.6.refs_0_), channel_id=1, source_target_pairs={{416,384},{448,416},{480,448},{0,480},{32,0},{64,32},{96,64},{417,... | collective-permute-start | bytes 417800 | tf_op jit(solution)/shard_map/ppermute | solution.py:305
  51.4 2.0 collective-permute-done.8.refs_0_
  53.4 0.7 collective-permute-start.9
  54.0 5.6 %collective-permute-start.10 = (bf16[136,512]{1,0:T(8,128)(2,1)S(1)}, bf16[136,512]{1,0:T(8,128)(2,1)S(1)}, u32[]{:S(2)}, u32[]{:S(2)}) collective-permute-start(bf16[136,512]{1,0:T(8,128)(2,1)S(1)} %collective-permute-done.8.refs_0_), channel_id=1, source_target_pairs={{384,352},{416,384},{448,416},{480,448},{0,480},{32,0},{64,32},{38... | collective-permute-start | bytes 417800 | tf_op jit(solution)/shard_map/ppermute | solution.py:305
  59.7 2.0 collective-permute-done.10.refs_0_
  61.7 0.7 collective-permute-start.11
  62.3 5.6 %collective-permute-start.12 = (bf16[136,512]{1,0:T(8,128)(2,1)S(1)}, bf16[136,512]{1,0:T(8,128)(2,1)S(1)}, u32[]{:S(2)}, u32[]{:S(2)}) collective-permute-start(bf16[136,512]{1,0:T(8,128)(2,1)S(1)} %collective-permute-done.10.refs_0_), channel_id=1, source_target_pairs={{352,320},{384,352},{416,384},{448,416},{480,448},{0,480},{32,0},{... | collective-permute-start | bytes 417800 | tf_op jit(solution)/shard_map/ppermute | solution.py:305
  68.0 2.0 collective-permute-done.12.refs_0_
  70.0 0.7 collective-permute-start.13
  70.6 5.6 %collective-permute-start.14 = (bf16[136,512]{1,0:T(8,128)(2,1)S(1)}, bf16[136,512]{1,0:T(8,128)(2,1)S(1)}, u32[]{:S(2)}, u32[]{:S(2)}) collective-permute-start(bf16[136,512]{1,0:T(8,128)(2,1)S(1)} %collective-permute-done.12.refs_0_), channel_id=1, source_target_pairs={{320,288},{352,320},{384,352},{416,384},{448,416},{480,448},{0,480... | collective-permute-start | bytes 417800 | tf_op jit(solution)/shard_map/ppermute | solution.py:305
  76.3 1.9 collective-permute-done.14.refs_0_
  78.3 0.7 collective-permute-start.15
  78.9 0.2 shard_map.153
  79.2 8.5 %collective-permute-start.16 = (f32[80,512]{1,0:T(8,128)S(1)}, f32[80,512]{1,0:T(8,128)S(1)}, u32[]{:S(2)}, u32[]{:S(2)}) collective-permute-start(f32[80,512]{1,0:T(8,128)S(1)} %get-tuple-element.79), channel_id=1, source_target_pairs={{0,16},{16,0},{1,17},{17,1},{2,18},{18,2},{3,19},{19,3},{4,20},{20... | collective-permute-start | bytes 491528 | tf_op jit(solution)/shard_map/ppermute | solution.py:316
  87.7 1.0 collective-permute-done.16.other_ref
  88.8 23.4 %all_to_all.35 = bf16[16,64,512]{2,1,0:T(8,128)(2,1)S(1)} all-to-all(bf16[16,64,512]{2,1,0:T(8,128)(2,1)S(1)} %shard_map.155), channel_id=1, replica_groups=mesh['z'=16,'c'=2,'y'=4,'x'=4] {'y','x'}, dimensions={0} | all-to-all | bytes 2097152 | tf_op jit(solution)/shard_map/all_to_all | solution.py:247
  112.3 1.0 shard_map.156
  113.2 3.5 %all-to-all-start.2 = ((f32[16,1,512]{2,1,0:T(1,128)}), f32[16,1,512]{2,1,0:T(1,128)S(1)}, u32[]{:S(2)}, u32[]{:S(2)}) async-start(f32[16,1,512]{2,1,0:T(1,128)} %get-tuple-element.83), calls=%async_computation.2 | async-start | bytes 65536 | tf_op jit(solution)/shard_map/all_to_all | solution.py:247
  116.8 6.3 %all-to-all-done.2.refs_1_ = f32[16,1,512]{2,1,0:T(1,128)S(1)} async-done(((f32[16,1,512]{2,1,0:T(1,128)}), f32[16,1,512]{2,1,0:T(1,128)S(1)}, u32[]{:S(2)}, u32[]{:S(2)}) %all-to-all-start.2) | async-done | bytes 32800 | tf_op jit(solution)/shard_map/all_to_all | solution.py:247
  123.1 0.7 shard_map.157
  123.9 46.4 %all_to_all.36 = bf16[32,40,128]{2,1,0:T(8,128)(2,1)S(1)} all-to-all(bf16[32,40,128]{2,1,0:T(8,128)(2,1)S(1)} %bitcast.46), channel_id=1, replica_groups=mesh['z'=16,'c'=2,'y'=4,'x'=4] {'z','c'}, dimensions={0} | all-to-all | bytes 655360 | tf_op jit(solution)/shard_map/all_to_all | solution.py:247
  170.2 0.4 shard_map.158
  170.7 27.6 %all_to_all.37.rows_ref = bf16[16,448,128]{2,1,0:T(8,128)(2,1)S(1)} all-to-all(bf16[16,448,128]{2,1,0:T(8,128)(2,1)S(1)} %shard_map.158), channel_id=1, replica_groups=mesh['z'=16,'c'=2,'y'=4,'x'=4] {'y','x'}, dimensions={0} | all-to-all | bytes 3670016 | tf_op jit(solution)/shard_map/all_to_all | solution.py:247
  198.2 0.9 shard_map.159
  199.2 27.4 %all_to_all.38.hidden_ref = bf16[16,448,128]{2,1,0:T(8,128)(2,1)S(1)} all-to-all(bf16[16,448,128]{2,1,0:T(8,128)(2,1)S(1)} %shard_map.159), channel_id=1, replica_groups=mesh['z'=16,'c'=2,'y'=4,'x'=4] {'y','x'}, dimensions={0} | all-to-all | bytes 3670016 | tf_op jit(solution)/shard_map/all_to_all | solution.py:247
  226.6 0.9 shard_map.160
  227.5 31.4 %all_to_all.39 = bf16[32,40,128]{2,1,0:T(8,128)(2,1)S(1)} all-to-all(bf16[32,40,128]{2,1,0:T(8,128)(2,1)S(1)} %bitcast.47), channel_id=1, replica_groups=mesh['z'=16,'c'=2,'y'=4,'x'=4] {'z','c'}, dimensions={0} | all-to-all | bytes 655360 | tf_op jit(solution)/shard_map/all_to_all | solution.py:247
  258.9 1.4 shard_map.161
  (54 shorter events, 1.0 us)
Async XLA Ops:
  0.0 1.5 copy-start.7
  0.0 1.5 copy-start.8
  3.2 5.0 %copy-start.12 = (f32[512,1]{0,1:T(1,128)S(1)}, f32[512,1]{0,1:T(1,128)}, u32[]{:S(2)}) copy-start(f32[512,1]{0,1:T(1,128)} %param.18) | copy-start | bytes 6148
  3.2 5.0 %copy-start.11 = (bf16[512,64]{0,1:T(8,128)(2,1)S(1)}, bf16[512,64]{0,1:T(8,128)(2,1)}, u32[]{:S(2)}) copy-start(bf16[512,64]{0,1:T(8,128)(2,1)} %param.15) | copy-start | bytes 196612
  3.2 12.6 %copy-start.9 = (bf16[512,64]{0,1:T(8,128)(2,1)S(1)}, bf16[512,64]{0,1:T(8,128)(2,1)}, u32[]{:S(2)}) copy-start(bf16[512,64]{0,1:T(8,128)(2,1)} %param.16) | copy-start | bytes 196612
  3.2 12.6 %copy-start.10 = (bf16[512,64]{0,1:T(8,128)(2,1)S(1)}, bf16[512,64]{0,1:T(8,128)(2,1)}, u32[]{:S(2)}) copy-start(bf16[512,64]{0,1:T(8,128)(2,1)} %param.17) | copy-start | bytes 196612
  3.2 40.9 %all-to-all-start = ((bf16[4,128,2048]{2,1,0:T(8,128)(2,1)}), bf16[4,128,2048]{2,1,0:T(8,128)(2,1)S(1)}, u32[]{:S(2)}, u32[]{:S(2)}) async-start(bf16[4,128,2048]{2,1,0:T(8,128)(2,1)} %pad_maximum_fusion), calls=%async_computation | async-start | bytes 4194304 | tf_op jit(solution)/shard_map/all_to_all | solution.py:247
  8.3 15.4 %collective-permute-start.2 = (bf16[72,512]{1,0:T(8,128)(2,1)S(1)}, bf16[72,512]{1,0:T(8,128)(2,1)S(1)}, u32[]{:S(2)}, u32[]{:S(2)}) collective-permute-start(bf16[72,512]{1,0:T(8,128)(2,1)S(1)} %concatenate.22), channel_id=1, source_target_pairs={{0,16},{16,0},{1,17},{17,1},{2,18},{18,2},{3,19},{19,3},{4,20},{20... | collective-permute-start | bytes 221192 | tf_op jit(solution)/shard_map/ppermute | solution.py:278
  15.9 9.4 %collective-permute-start.1 = (bf16[136,512]{1,0:T(8,128)(2,1)S(1)}, bf16[136,512]{1,0:T(8,128)(2,1)S(1)}, u32[]{:S(2)}, u32[]{:S(2)}) collective-permute-start(bf16[136,512]{1,0:T(8,128)(2,1)S(1)} %concatenate.21.block_ref), channel_id=1, source_target_pairs={{0,480},{32,0},{64,32},{96,64},{128,96},{160,128},{192,160},{1,481... | collective-permute-start | bytes 417800 | tf_op jit(solution)/shard_map/ppermute | solution.py:305
  22.4 4.3 %collective-permute-start = (bf16[136,512]{1,0:T(8,128)(2,1)S(1)}, bf16[136,512]{1,0:T(8,128)(2,1)S(1)}, u32[]{:S(2)}, u32[]{:S(2)}) collective-permute-start(bf16[136,512]{1,0:T(8,128)(2,1)S(1)} %concatenate.21.block_ref), channel_id=1, source_target_pairs={{0,32},{32,64},{64,96},{96,128},{128,160},{160,192},{192,224},{224... | collective-permute-start | bytes 417800 | tf_op jit(solution)/shard_map/ppermute | solution.py:309
  26.7 6.2 %collective-permute-start.3 = (bf16[136,512]{1,0:T(8,128)(2,1)S(1)}, bf16[136,512]{1,0:T(8,128)(2,1)S(1)}, u32[]{:S(2)}, u32[]{:S(2)}) collective-permute-start(bf16[136,512]{1,0:T(8,128)(2,1)S(1)} %collective-permute-done.refs_1_), channel_id=1, source_target_pairs={{32,64},{64,96},{96,128},{128,160},{160,192},{192,224},{224,256},{... | collective-permute-start | bytes 417800 | tf_op jit(solution)/shard_map/ppermute | solution.py:309
  27.3 7.9 %collective-permute-start.4 = (bf16[136,512]{1,0:T(8,128)(2,1)S(1)}, bf16[136,512]{1,0:T(8,128)(2,1)S(1)}, u32[]{:S(2)}, u32[]{:S(2)}) collective-permute-start(bf16[136,512]{1,0:T(8,128)(2,1)S(1)} %collective-permute-done.1.refs_0_), channel_id=1, source_target_pairs={{480,448},{0,480},{32,0},{64,32},{96,64},{128,96},{160,128},{481,4... | collective-permute-start | bytes 417800 | tf_op jit(solution)/shard_map/ppermute | solution.py:305
  32.1 10.5 %copy-start.6 = (bf16[1024,128]{1,0:T(8,128)(2,1)S(1)}, bf16[1024,128]{1,0:T(8,128)(2,1)}, u32[]{:S(2)}) copy-start(bf16[1024,128]{1,0:T(8,128)(2,1)} %param.20) | copy-start | bytes 786436
  32.1 10.7 %copy-start.2 = (s32[512,2]{0,1:T(2,128)S(1)}, s32[512,2]{0,1:T(2,128)}, u32[]{:S(2)}) copy-start(s32[512,2]{0,1:T(2,128)} %param.22) | copy-start | bytes 12292
  32.1 0.7 copy-start.4
  35.2 8.9 %collective-permute-start.5 = (bf16[136,512]{1,0:T(8,128)(2,1)S(1)}, bf16[136,512]{1,0:T(8,128)(2,1)S(1)}, u32[]{:S(2)}, u32[]{:S(2)}) collective-permute-start(bf16[136,512]{1,0:T(8,128)(2,1)S(1)} %collective-permute-done.3.refs_1_), channel_id=1, source_target_pairs={{64,96},{96,128},{128,160},{160,192},{192,224},{224,256},{256,288}... | collective-permute-start | bytes 417800 | tf_op jit(solution)/shard_map/ppermute | solution.py:309
  35.9 8.2 %collective-permute-start.6 = (bf16[136,512]{1,0:T(8,128)(2,1)S(1)}, bf16[136,512]{1,0:T(8,128)(2,1)S(1)}, u32[]{:S(2)}, u32[]{:S(2)}) collective-permute-start(bf16[136,512]{1,0:T(8,128)(2,1)S(1)} %collective-permute-done.4.refs_0_), channel_id=1, source_target_pairs={{448,416},{480,448},{0,480},{32,0},{64,32},{96,64},{128,96},{449,4... | collective-permute-start | bytes 417800 | tf_op jit(solution)/shard_map/ppermute | solution.py:305
  43.1 1.0 copy-start.5
  44.1 7.3 %collective-permute-start.7 = (bf16[136,512]{1,0:T(8,128)(2,1)S(1)}, bf16[136,512]{1,0:T(8,128)(2,1)S(1)}, u32[]{:S(2)}, u32[]{:S(2)}) collective-permute-start(bf16[136,512]{1,0:T(8,128)(2,1)S(1)} %collective-permute-done.5.refs_1_), channel_id=1, source_target_pairs={{96,128},{128,160},{160,192},{192,224},{224,256},{256,288},{288,32... | collective-permute-start | bytes 417800 | tf_op jit(solution)/shard_map/ppermute | solution.py:309
  44.8 8.6 %collective-permute-start.8 = (bf16[136,512]{1,0:T(8,128)(2,1)S(1)}, bf16[136,512]{1,0:T(8,128)(2,1)S(1)}, u32[]{:S(2)}, u32[]{:S(2)}) collective-permute-start(bf16[136,512]{1,0:T(8,128)(2,1)S(1)} %collective-permute-done.6.refs_0_), channel_id=1, source_target_pairs={{416,384},{448,416},{480,448},{0,480},{32,0},{64,32},{96,64},{417,... | collective-permute-start | bytes 417800 | tf_op jit(solution)/shard_map/ppermute | solution.py:305
  53.4 6.3 %collective-permute-start.9 = (bf16[136,512]{1,0:T(8,128)(2,1)S(1)}, bf16[136,512]{1,0:T(8,128)(2,1)S(1)}, u32[]{:S(2)}, u32[]{:S(2)}) collective-permute-start(bf16[136,512]{1,0:T(8,128)(2,1)S(1)} %collective-permute-done.7.refs_1_), channel_id=1, source_target_pairs={{128,160},{160,192},{192,224},{224,256},{256,288},{288,320},{320,3... | collective-permute-start | bytes 417800 | tf_op jit(solution)/shard_map/ppermute | solution.py:309
  54.0 7.6 %collective-permute-start.10 = (bf16[136,512]{1,0:T(8,128)(2,1)S(1)}, bf16[136,512]{1,0:T(8,128)(2,1)S(1)}, u32[]{:S(2)}, u32[]{:S(2)}) collective-permute-start(bf16[136,512]{1,0:T(8,128)(2,1)S(1)} %collective-permute-done.8.refs_0_), channel_id=1, source_target_pairs={{384,352},{416,384},{448,416},{480,448},{0,480},{32,0},{64,32},{38... | collective-permute-start | bytes 417800 | tf_op jit(solution)/shard_map/ppermute | solution.py:305
  61.7 6.3 %collective-permute-start.11 = (bf16[136,512]{1,0:T(8,128)(2,1)S(1)}, bf16[136,512]{1,0:T(8,128)(2,1)S(1)}, u32[]{:S(2)}, u32[]{:S(2)}) collective-permute-start(bf16[136,512]{1,0:T(8,128)(2,1)S(1)} %collective-permute-done.9.refs_1_), channel_id=1, source_target_pairs={{160,192},{192,224},{224,256},{256,288},{288,320},{320,352},{352,3... | collective-permute-start | bytes 417800 | tf_op jit(solution)/shard_map/ppermute | solution.py:309
  62.3 7.6 %collective-permute-start.12 = (bf16[136,512]{1,0:T(8,128)(2,1)S(1)}, bf16[136,512]{1,0:T(8,128)(2,1)S(1)}, u32[]{:S(2)}, u32[]{:S(2)}) collective-permute-start(bf16[136,512]{1,0:T(8,128)(2,1)S(1)} %collective-permute-done.10.refs_0_), channel_id=1, source_target_pairs={{352,320},{384,352},{416,384},{448,416},{480,448},{0,480},{32,0},{... | collective-permute-start | bytes 417800 | tf_op jit(solution)/shard_map/ppermute | solution.py:305
  70.0 6.3 %collective-permute-start.13 = (bf16[136,512]{1,0:T(8,128)(2,1)S(1)}, bf16[136,512]{1,0:T(8,128)(2,1)S(1)}, u32[]{:S(2)}, u32[]{:S(2)}) collective-permute-start(bf16[136,512]{1,0:T(8,128)(2,1)S(1)} %collective-permute-done.11.refs_1_), channel_id=1, source_target_pairs={{192,224},{224,256},{256,288},{288,320},{320,352},{352,384},{384,4... | collective-permute-start | bytes 417800 | tf_op jit(solution)/shard_map/ppermute | solution.py:309
  70.6 7.6 %collective-permute-start.14 = (bf16[136,512]{1,0:T(8,128)(2,1)S(1)}, bf16[136,512]{1,0:T(8,128)(2,1)S(1)}, u32[]{:S(2)}, u32[]{:S(2)}) collective-permute-start(bf16[136,512]{1,0:T(8,128)(2,1)S(1)} %collective-permute-done.12.refs_0_), channel_id=1, source_target_pairs={{320,288},{352,320},{384,352},{416,384},{448,416},{480,448},{0,480... | collective-permute-start | bytes 417800 | tf_op jit(solution)/shard_map/ppermute | solution.py:305
  78.3 0.9 collective-permute-start.15
  79.2 9.5 %collective-permute-start.16 = (f32[80,512]{1,0:T(8,128)S(1)}, f32[80,512]{1,0:T(8,128)S(1)}, u32[]{:S(2)}, u32[]{:S(2)}) collective-permute-start(f32[80,512]{1,0:T(8,128)S(1)} %get-tuple-element.79), channel_id=1, source_target_pairs={{0,16},{16,0},{1,17},{17,1},{2,18},{18,2},{3,19},{19,3},{4,20},{20... | collective-permute-start | bytes 491528 | tf_op jit(solution)/shard_map/ppermute | solution.py:316
  113.2 9.9 %all-to-all-start.2 = ((f32[16,1,512]{2,1,0:T(1,128)}), f32[16,1,512]{2,1,0:T(1,128)S(1)}, u32[]{:S(2)}, u32[]{:S(2)}) async-start(f32[16,1,512]{2,1,0:T(1,128)} %get-tuple-element.83), calls=%async_computation.2 | async-start | bytes 65536 | tf_op jit(solution)/shard_map/all_to_all | solution.py:247
  199.2 27.4 %copy-start = (bf16[4,512,128]{2,1,0:T(8,128)(2,1)S(1)}, bf16[4,512,128]{2,1,0:T(8,128)(2,1)}, u32[]{:S(2)}) copy-start(bf16[4,512,128]{2,1,0:T(8,128)(2,1)} %weight_ref.1) | copy-start | bytes 1572868
  199.2 27.4 %copy-start.1 = (bf16[512,128]{1,0:T(8,128)(2,1)S(1)}, bf16[512,128]{1,0:T(8,128)(2,1)}, u32[]{:S(2)}) copy-start(bf16[512,128]{1,0:T(8,128)(2,1)} %shared_ref.1) | copy-start | bytes 393220
  226.6 32.3 %copy-start.3 = (f32[512,2]{0,1:T(2,128)S(1)}, f32[512,2]{0,1:T(2,128)}, u32[]{:S(2)}) copy-start(f32[512,2]{0,1:T(2,128)} %param.23) | copy-start | bytes 12292

commit v4 on v3

--- a/solution.py
+++ b/solution.py
@@ -124,34 +124,24 @@
         used = used + jnp.sum(hot, axis=1, keepdims=True)
 
 
-def mid_kernel(heads_ref, weight_ref, residual_ref, mid_ref, squares_ref):
-    projected = dot(weight_ref[...], heads_ref[...])
-    mid = (residual_ref[...].astype(F32) + projected).astype(BF)
-    mid_ref[...] = mid
-    wide = mid.astype(F32)
-    squares_ref[...] = jnp.broadcast_to(
-        jnp.sum(wide * wide, axis=0, keepdims=True)[None], squares_ref.shape
-    )
-
-
 def hot_slots(targets_ref, k, first, rows):
     tokens = targets_ref.shape[1]
     slot_at = lax.broadcasted_iota(jnp.int32, (rows, tokens), 0) + first
     return targets_ref[k : k + 1] == slot_at
 
 
-def normed_kernel(width, mid_ref, squares_ref, gain_ref, targets_ref, rows_ref, normed_ref):
-    total = jnp.sum(squares_ref[...], axis=0)
-    inverse = lax.rsqrt(total / width + EPSILON)
-    normed = (mid_ref[...].astype(F32) * inverse * gain_ref[...]).astype(BF)
-    normed_ref[...] = normed.astype(F32).T.astype(BF)
+def mid_kernel(heads_ref, weight_ref, residual_ref, targets_ref, mid_ref, rows_ref, own_ref):
+    projected = dot(weight_ref[...], heads_ref[...])
+    mid = (residual_ref[...].astype(F32) + projected).astype(BF)
+    mid_ref[...] = mid
+    own_ref[...] = mid.astype(F32).T.astype(BF)
     chunk = rows_ref.shape[0] // 4
     for part in range(4):
         hot = hot_slots(targets_ref, 0, part * chunk, chunk) | hot_slots(
             targets_ref, 1, part * chunk, chunk
         )
         rows_ref[part * chunk : (part + 1) * chunk] = dot(
-            hot.astype(F32).astype(BF), normed, NT
+            hot.astype(F32).astype(BF), mid, NT
         ).astype(BF)
 
 
@@ -166,7 +156,7 @@
     return (frm == src * 40 + el * 10 + within - src * 10).astype(F32).astype(BF)
 
 
-def spread_kernel(arrived_ref, normed_ref, out_ref):
+def spread_kernel(arrived_ref, own_ref, out_ref):
     order = sorting()
     for group in range(4):
         rows = dot(order, arrived_ref[group * 320 : (group + 1) * 320]).astype(BF)
@@ -175,12 +165,23 @@
             for y in range(4):
                 out_ref[y * 4 + el, group * 80 : (group + 1) * 80] = piece
     for x in range(4):
-        piece = normed_ref[x * 128 : (x + 1) * 128]
+        piece = own_ref[x * 128 : (x + 1) * 128]
         for y in range(4):
             out_ref[y * 4 + x, 320:448] = piece
 
 
-def hidden_kernel(rows_ref, weight_ref, out_ref):
+def hidden_kernel(rows_ref, weight_ref, gain_ref, out_ref):
+    squares = jnp.zeros(rows_ref.shape[1:], F32)
+    for t in range(16):
+        wide = rows_ref[t].astype(F32)
+        squares = squares + wide * wide
+    total = jnp.sum(squares, axis=1, keepdims=True)
+    inverse = lax.rsqrt(total / gain_ref.shape[1] + EPSILON)
+
+    def normed(t):
+        gain = gain_ref[:, t * 128 : (t + 1) * 128].astype(F32)
+        return (rows_ref[t].astype(F32) * inverse * gain).astype(BF)
+
     expert = jnp.zeros((320, 256), F32)
     shared = jnp.zeros((128, 256), F32)
 
@@ -191,7 +192,7 @@
 
     for t in range(0, 16, 2):
         cols = slice(t * 128, (t + 2) * 128)
-        rows = jnp.concatenate([rows_ref[t], rows_ref[t + 1]], axis=1)
+        rows = jnp.concatenate([normed(t), normed(t + 1)], axis=1)
         expert = expert + dot(rows[0:320], weights(0, cols), NT)
         shared = shared + dot(rows[320:448], weights(64, cols), NT)
     for first, count, both in ((0, 320, expert), (320, 128, shared)):
@@ -282,21 +283,22 @@
     local = jnp.stack([expert_gate, expert_up], axis=1).transpose(0, 1, 3, 2).reshape(4, 64, width)
     both = jnp.concatenate([shared_gate.T, shared_up.T], axis=0)
     local = jnp.concatenate([local, jnp.broadcast_to(both[None], (4, 64, width))], axis=1)
-    up_weight = exchange(local, "x")
     targets = call(slots_kernel, shape((2, tokens), jnp.int32), routes.T)
-    at = (lax.axis_index("y") * 4 + lax.axis_index("x")) * 128
     out_rows, residual = out_weight.T, residual.T
-    gain = lax.dynamic_slice_in_dim(norm_gain, at, 128, 0).astype(F32)[:, None]
-
-    prepared = (up_weight, targets, out_rows, residual, gain)
+    gain = norm_gain.astype(F32)[None]
+    prepared = (targets, out_rows, residual, gain)
 
     up = down = block
     top, acc = call(own_kernel, state, c.reshape(1), block, query, smem=1)
     before = now = (top, acc)
     chip = z.reshape(1)
     for k in range(1, chips // 2 + 1):
-        if k == 4:
+        if k == 2:
+            up, down, before, local = lax.optimization_barrier((up, down, before, local))
+        elif k == 5:
             up, down, before, prepared = lax.optimization_barrier((up, down, before, prepared))
+        elif k == 6:
+            up, down, before, up_weight = lax.optimization_barrier((up, down, before, up_weight))
         elif k > 1:
             up, down, before = lax.optimization_barrier((up, down, before))
         arrived, outs = [], state
@@ -308,34 +310,28 @@
             outs = (*state, shape((80, tokens), F32))
         up = lax.ppermute(up, "z", [(i, i + 1) for i in range(k - 1, chips - 1)])
         arrived.append(up)
+        if k == 2:
+            up_weight = exchange(local, "x")
         kernel = functools.partial(past_kernel, k, chips, len(arrived))
         before = now
         now = call(kernel, outs, chip, *arrived, query, *now, smem=1, flops=2**30)
     top, acc, sent = now
-    up_weight, targets, out_rows, residual, gain = prepared
+    targets, out_rows, residual, gain = prepared
     other = lax.ppermute(sent, "c", ((0, 1), (1, 0)))
     heads = call(merge_kernel, shape((16, HDIM, tokens)), top, acc, other)
     heads = exchange(heads, tp)
 
-    mid, squares = call(
+    mid, rows, own = call(
         mid_kernel,
-        (shape((128, tokens)), shape((16, 1, tokens), F32)),
+        (shape((128, tokens)), shape((1280, 128)), shape((tokens, 128))),
         heads.reshape(16 * HDIM, tokens),
         out_rows,
         residual,
-    )
-    squares = exchange(squares, tp)
-    rows, normed = call(
-        lambda *refs: normed_kernel(width, *refs),
-        (shape((1280, 128)), shape((tokens, 128))),
-        mid,
-        squares,
-        gain,
         targets,
     )
     arrived = exchange(rows.reshape(32, 40, 128), ("z", "c")).reshape(1280, 128)
-    spread = exchange(call(spread_kernel, shape((16, 448, 128)), arrived, normed), tp)
-    hidden = exchange(call(hidden_kernel, shape((16, 448, 128)), spread, up_weight), tp)
+    spread = exchange(call(spread_kernel, shape((16, 448, 128)), arrived, own), tp)
+    hidden = exchange(call(hidden_kernel, shape((16, 448, 128)), spread, up_weight, gain), tp)
     produced, shared = call(
         down_kernel,
         (shape((1280, 128)), shape((tokens, 128), F32)),

time: 261 us -> 248 us (0.950)
  waiting for transfers between devices: 19.9 us -> 10.7 us
  starting transfers between devices: 69.9 us -> 62.5 us
  local copies, waits for them, and re-layouts: 3.3 us -> 7.46 us
    all_to_all x2 -> x1, waiting for transfers between devices: 6.29 us -> 0.01 us  [exchange(): return lax.all_to_all(array, axis, split_axis=0, concat_axis=0, tiled=True)]
    ppermute x1, starting transfers between devices: 7.54 us -> 2.86 us  [shards(): lax.ppermute(query, 'c', ((0, 1), (1, 0)))]
    all_to_all x2 -> x1, starting transfers between devices: 8.47 us -> 4.03 us  [exchange(): return lax.all_to_all(array, axis, split_axis=0, concat_axis=0, tiled=True)]
    unnamed x28 -> x24, local copies, waits for them, and re-layouts: 2.89 us -> 5.48 us
    pallas_call x17 -> x16, Pallas kernels: 6.84 us -> 6.39 us  [call(): pl.pallas_call(kernel, out_shape=outs, in_specs=specs, out_specs=jax.tree...]
  transfers between devices with their start and end apart: 19 -> 18, of which waited for: 9 -> 6; matrix products, arithmetic and copies ran while one was open for 1% -> 2% of each run, Pallas kernels for 0% -> 1%
where the time goes in v4:
time: 248 us; the launch traced here: 247 us
  blocking collectives  155 us (62%)
  starting transfers between devices  62.5 us (25%)
  waiting for transfers between devices  10.7 us (4%)
  local copies, waits for them, and re-layouts  7.46 us (3%)
  Pallas kernels  6.39 us (3%)
  other arithmetic  4.48 us (2%)
    all_to_all x5, blocking collectives, exchange(): return lax.all_to_all(array, axis, split_axis=0, concat_axis=0, tiled=True)  155 us
    ppermute x7, starting transfers between devices, shards(): down = lax.ppermute(down, 'z', back)  41.5 us
    ppermute x7, waiting for transfers between devices, shards(): down = lax.ppermute(down, 'z', back)  9.66 us
    ppermute x1, starting transfers between devices, shards(): other = lax.ppermute(sent, 'c', ((0, 1), (1, 0)))  8.01 us
    pallas_call x16, Pallas kernels, call(): pl.pallas_call(kernel, out_shape=outs, in_specs=specs, out_specs=jax.tree...  6.39 us
    ppermute x8, starting transfers between devices, shards(): up = lax.ppermute(up, 'z', [(i, i + 1) for i in range(k - 1, chips - 1)])  6.05 us
    unnamed x24, local copies, waits for them, and re-layouts  5.48 us
  transfers between devices with their start and end apart: 18, of which 6 were waited for; matrix products, arithmetic and copies ran while one was open for 2% of the time, Pallas kernels for 1%

profile of v4, /device:TPU:1, one launch (start us, length us, event | category | flops | bytes accessed | tf_op | source)
XLA Modules:
  0.0 247.2 jit_solution(11661293715560594270)
XLA Ops:
  0.0 0.7 fusion.3
  0.7 1.7 concatenate.21.block_ref
  2.4 11.9 %collective-permute-start.1 = (bf16[136,512]{1,0:T(8,128)(2,1)S(1)}, bf16[136,512]{1,0:T(8,128)(2,1)S(1)}, u32[]{:S(2)}, u32[]{:S(2)}) collective-permute-start(bf16[136,512]{1,0:T(8,128)(2,1)S(1)} %concatenate.21.block_ref), channel_id=1, source_target_pairs={{0,480},{32,0},{64,32},{96,64},{128,96},{160,128},{192,160},{1,481... | collective-permute-start | bytes 417800 | tf_op jit(solution)/shard_map/ppermute | solution.py:307
  14.4 1.3 collective-permute-start
  15.7 0.8 multiply_bitcast_fusion
  16.6 2.9 %collective-permute-start.2 = (bf16[72,512]{1,0:T(8,128)(2,1)S(1)}, bf16[72,512]{1,0:T(8,128)(2,1)S(1)}, u32[]{:S(2)}, u32[]{:S(2)}) collective-permute-start(bf16[72,512]{1,0:T(8,128)(2,1)S(1)} %concatenate.22), channel_id=1, source_target_pairs={{0,16},{16,0},{1,17},{17,1},{2,18},{18,2},{3,19},{19,3},{4,20},{20... | collective-permute-start | bytes 221192 | tf_op jit(solution)/shard_map/ppermute | solution.py:279
  19.5 1.3 maximum_bitcast_fusion
  21.1 1.6 pad_maximum_fusion
  22.7 0.6 shard_map.145
  23.3 4.0 %all-to-all-start = ((bf16[4,128,2048]{2,1,0:T(8,128)(2,1)}), bf16[4,128,2048]{2,1,0:T(8,128)(2,1)S(1)}, u32[]{:S(2)}, u32[]{:S(2)}) async-start(bf16[4,128,2048]{2,1,0:T(8,128)(2,1)} %pad_maximum_fusion), calls=%async_computation | async-start | bytes 4194304 | tf_op jit(solution)/shard_map/all_to_all | solution.py:248
  27.3 0.7 collective-permute-start.3
  27.9 1.9 collective-permute-start.4
  29.9 4.2 %collective-permute-done.4.refs_0_ = bf16[136,512]{1,0:T(8,128)(2,1)S(1)} collective-permute-done((bf16[136,512]{1,0:T(8,128)(2,1)S(1)}, bf16[136,512]{1,0:T(8,128)(2,1)S(1)}, u32[]{:S(2)}, u32[]{:S(2)}) %collective-permute-start.4) | collective-permute-done | bytes 139296 | tf_op jit(solution)/shard_map/ppermute | solution.py:307
  34.1 0.8 collective-permute-start.5
  34.9 4.0 %collective-permute-start.6 = (bf16[136,512]{1,0:T(8,128)(2,1)S(1)}, bf16[136,512]{1,0:T(8,128)(2,1)S(1)}, u32[]{:S(2)}, u32[]{:S(2)}) collective-permute-start(bf16[136,512]{1,0:T(8,128)(2,1)S(1)} %collective-permute-done.4.refs_0_), channel_id=1, source_target_pairs={{448,416},{480,448},{0,480},{32,0},{64,32},{96,64},{128,96},{449,4... | collective-permute-start | bytes 417800 | tf_op jit(solution)/shard_map/ppermute | solution.py:307
  39.0 0.7 copy-done.6
  39.7 1.3 collective-permute-done.6.refs_0_
  41.0 0.7 collective-permute-start.7
  41.7 5.9 %collective-permute-start.8 = (bf16[136,512]{1,0:T(8,128)(2,1)S(1)}, bf16[136,512]{1,0:T(8,128)(2,1)S(1)}, u32[]{:S(2)}, u32[]{:S(2)}) collective-permute-start(bf16[136,512]{1,0:T(8,128)(2,1)S(1)} %collective-permute-done.6.refs_0_), channel_id=1, source_target_pairs={{416,384},{448,416},{480,448},{0,480},{32,0},{64,32},{96,64},{417,... | collective-permute-start | bytes 417800 | tf_op jit(solution)/shard_map/ppermute | solution.py:307
  47.6 1.0 copy.18
  48.6 1.1 copy.17
  49.7 0.3 shard_map.149.targets_ref
  50.0 1.0 copy-done.7
  51.0 0.7 collective-permute-start.9
  51.7 6.5 %collective-permute-start.10 = (bf16[136,512]{1,0:T(8,128)(2,1)S(1)}, bf16[136,512]{1,0:T(8,128)(2,1)S(1)}, u32[]{:S(2)}, u32[]{:S(2)}) collective-permute-start(bf16[136,512]{1,0:T(8,128)(2,1)S(1)} %collective-permute-done.8.refs_0_), channel_id=1, source_target_pairs={{384,352},{416,384},{448,416},{480,448},{0,480},{32,0},{64,32},{38... | collective-permute-start | bytes 417800 | tf_op jit(solution)/shard_map/ppermute | solution.py:307
  58.3 0.7 copy-done.4
  59.0 1.2 collective-permute-done.10.refs_0_
  60.3 0.7 collective-permute-start.11
  60.9 5.6 %collective-permute-start.12 = (bf16[136,512]{1,0:T(8,128)(2,1)S(1)}, bf16[136,512]{1,0:T(8,128)(2,1)S(1)}, u32[]{:S(2)}, u32[]{:S(2)}) collective-permute-start(bf16[136,512]{1,0:T(8,128)(2,1)S(1)} %collective-permute-done.10.refs_0_), channel_id=1, source_target_pairs={{352,320},{384,352},{416,384},{448,416},{480,448},{0,480},{32,0},{... | collective-permute-start | bytes 417800 | tf_op jit(solution)/shard_map/ppermute | solution.py:307
  66.6 1.0 copy-done.5
  67.6 1.0 collective-permute-done.12.refs_0_
  68.6 0.7 collective-permute-start.13
  69.2 5.6 %collective-permute-start.14 = (bf16[136,512]{1,0:T(8,128)(2,1)S(1)}, bf16[136,512]{1,0:T(8,128)(2,1)S(1)}, u32[]{:S(2)}, u32[]{:S(2)}) collective-permute-start(bf16[136,512]{1,0:T(8,128)(2,1)S(1)} %collective-permute-done.12.refs_0_), channel_id=1, source_target_pairs={{320,288},{352,320},{384,352},{416,384},{448,416},{480,448},{0,480... | collective-permute-start | bytes 417800 | tf_op jit(solution)/shard_map/ppermute | solution.py:307
  74.9 1.9 collective-permute-done.14.refs_0_
  76.9 0.7 collective-permute-start.15
  77.5 0.2 shard_map.153
  77.8 8.0 %collective-permute-start.16 = (f32[80,512]{1,0:T(8,128)S(1)}, f32[80,512]{1,0:T(8,128)S(1)}, u32[]{:S(2)}, u32[]{:S(2)}) collective-permute-start(f32[80,512]{1,0:T(8,128)S(1)} %get-tuple-element.80), channel_id=1, source_target_pairs={{0,16},{16,0},{1,17},{17,1},{2,18},{18,2},{3,19},{19,3},{4,20},{20... | collective-permute-start | bytes 491528 | tf_op jit(solution)/shard_map/ppermute | solution.py:320
  85.8 1.0 collective-permute-done.16.other_ref
  87.0 23.1 %all_to_all.30 = bf16[16,64,512]{2,1,0:T(8,128)(2,1)S(1)} all-to-all(bf16[16,64,512]{2,1,0:T(8,128)(2,1)S(1)} %shard_map.155), channel_id=1, replica_groups=mesh['z'=16,'c'=2,'y'=4,'x'=4] {'y','x'}, dimensions={0} | all-to-all | bytes 2097152 | tf_op jit(solution)/shard_map/all_to_all | solution.py:248
  110.1 1.0 shard_map.156
  111.1 45.9 %all_to_all.31 = bf16[32,40,128]{2,1,0:T(8,128)(2,1)S(1)} all-to-all(bf16[32,40,128]{2,1,0:T(8,128)(2,1)S(1)} %bitcast.43), channel_id=1, replica_groups=mesh['z'=16,'c'=2,'y'=4,'x'=4] {'z','c'}, dimensions={0} | all-to-all | bytes 655360 | tf_op jit(solution)/shard_map/all_to_all | solution.py:248
  157.0 0.4 shard_map.157
  157.5 27.4 %all_to_all.32.rows_ref = bf16[16,448,128]{2,1,0:T(8,128)(2,1)S(1)} all-to-all(bf16[16,448,128]{2,1,0:T(8,128)(2,1)S(1)} %shard_map.157), channel_id=1, replica_groups=mesh['z'=16,'c'=2,'y'=4,'x'=4] {'y','x'}, dimensions={0} | all-to-all | bytes 3670016 | tf_op jit(solution)/shard_map/all_to_all | solution.py:248
  184.9 1.2 shard_map.158
  186.1 27.3 %all_to_all.33.hidden_ref = bf16[16,448,128]{2,1,0:T(8,128)(2,1)S(1)} all-to-all(bf16[16,448,128]{2,1,0:T(8,128)(2,1)S(1)} %shard_map.158), channel_id=1, replica_groups=mesh['z'=16,'c'=2,'y'=4,'x'=4] {'y','x'}, dimensions={0} | all-to-all | bytes 3670016 | tf_op jit(solution)/shard_map/all_to_all | solution.py:248
  213.5 1.0 shard_map.159
  214.4 31.4 %all_to_all.34 = bf16[32,40,128]{2,1,0:T(8,128)(2,1)S(1)} all-to-all(bf16[32,40,128]{2,1,0:T(8,128)(2,1)S(1)} %bitcast.45), channel_id=1, replica_groups=mesh['z'=16,'c'=2,'y'=4,'x'=4] {'z','c'}, dimensions={0} | all-to-all | bytes 655360 | tf_op jit(solution)/shard_map/all_to_all | solution.py:248
  245.8 1.4 shard_map.160
  (46 shorter events, 0.7 us)
Async XLA Ops:
  2.4 20.8 %collective-permute-start.1 = (bf16[136,512]{1,0:T(8,128)(2,1)S(1)}, bf16[136,512]{1,0:T(8,128)(2,1)S(1)}, u32[]{:S(2)}, u32[]{:S(2)}) collective-permute-start(bf16[136,512]{1,0:T(8,128)(2,1)S(1)} %concatenate.21.block_ref), channel_id=1, source_target_pairs={{0,480},{32,0},{64,32},{96,64},{128,96},{160,128},{192,160},{1,481... | collective-permute-start | bytes 417800 | tf_op jit(solution)/shard_map/ppermute | solution.py:307
  14.4 8.9 %collective-permute-start = (bf16[136,512]{1,0:T(8,128)(2,1)S(1)}, bf16[136,512]{1,0:T(8,128)(2,1)S(1)}, u32[]{:S(2)}, u32[]{:S(2)}) collective-permute-start(bf16[136,512]{1,0:T(8,128)(2,1)S(1)} %concatenate.21.block_ref), channel_id=1, source_target_pairs={{0,32},{32,64},{64,96},{96,128},{128,160},{160,192},{192,224},{224... | collective-permute-start | bytes 417800 | tf_op jit(solution)/shard_map/ppermute | solution.py:311
  16.6 6.1 %collective-permute-start.2 = (bf16[72,512]{1,0:T(8,128)(2,1)S(1)}, bf16[72,512]{1,0:T(8,128)(2,1)S(1)}, u32[]{:S(2)}, u32[]{:S(2)}) collective-permute-start(bf16[72,512]{1,0:T(8,128)(2,1)S(1)} %concatenate.22), channel_id=1, source_target_pairs={{0,16},{16,0},{1,17},{17,1},{2,18},{18,2},{3,19},{19,3},{4,20},{20... | collective-permute-start | bytes 221192 | tf_op jit(solution)/shard_map/ppermute | solution.py:279
  19.4 1.5 copy-start.8
  19.5 1.5 copy-start.9
  23.3 37.0 %all-to-all-start = ((bf16[4,128,2048]{2,1,0:T(8,128)(2,1)}), bf16[4,128,2048]{2,1,0:T(8,128)(2,1)S(1)}, u32[]{:S(2)}, u32[]{:S(2)}) async-start(bf16[4,128,2048]{2,1,0:T(8,128)(2,1)} %pad_maximum_fusion), calls=%async_computation | async-start | bytes 4194304 | tf_op jit(solution)/shard_map/all_to_all | solution.py:248
  27.3 2.6 %collective-permute-start.3 = (bf16[136,512]{1,0:T(8,128)(2,1)S(1)}, bf16[136,512]{1,0:T(8,128)(2,1)S(1)}, u32[]{:S(2)}, u32[]{:S(2)}) collective-permute-start(bf16[136,512]{1,0:T(8,128)(2,1)S(1)} %collective-permute-done.refs_1_), channel_id=1, source_target_pairs={{32,64},{64,96},{96,128},{128,160},{160,192},{192,224},{224,256},{... | collective-permute-start | bytes 417800 | tf_op jit(solution)/shard_map/ppermute | solution.py:311
  27.9 6.2 %collective-permute-start.4 = (bf16[136,512]{1,0:T(8,128)(2,1)S(1)}, bf16[136,512]{1,0:T(8,128)(2,1)S(1)}, u32[]{:S(2)}, u32[]{:S(2)}) collective-permute-start(bf16[136,512]{1,0:T(8,128)(2,1)S(1)} %collective-permute-done.1.refs_0_), channel_id=1, source_target_pairs={{480,448},{0,480},{32,0},{64,32},{96,64},{128,96},{160,128},{481,4... | collective-permute-start | bytes 417800 | tf_op jit(solution)/shard_map/ppermute | solution.py:307
  29.9 17.6 %copy-start.10 = (bf16[2048]{0:T(1024)(128)(2,1)S(1)}, bf16[2048]{0:T(1024)(128)(2,1)}, u32[]{:S(2)}) copy-start(bf16[2048]{0:T(1024)(128)(2,1)} %param.21) | copy-start | bytes 12292
  34.1 15.6 %copy-start.2 = (s32[512,2]{0,1:T(2,128)S(1)}, s32[512,2]{0,1:T(2,128)}, u32[]{:S(2)}) copy-start(s32[512,2]{0,1:T(2,128)} %param.22) | copy-start | bytes 12292
  34.1 5.6 %collective-permute-start.5 = (bf16[136,512]{1,0:T(8,128)(2,1)S(1)}, bf16[136,512]{1,0:T(8,128)(2,1)S(1)}, u32[]{:S(2)}, u32[]{:S(2)}) collective-permute-start(bf16[136,512]{1,0:T(8,128)(2,1)S(1)} %collective-permute-done.3.refs_1_), channel_id=1, source_target_pairs={{64,96},{96,128},{128,160},{160,192},{192,224},{224,256},{256,288}... | collective-permute-start | bytes 417800 | tf_op jit(solution)/shard_map/ppermute | solution.py:311
  34.9 6.1 %collective-permute-start.6 = (bf16[136,512]{1,0:T(8,128)(2,1)S(1)}, bf16[136,512]{1,0:T(8,128)(2,1)S(1)}, u32[]{:S(2)}, u32[]{:S(2)}) collective-permute-start(bf16[136,512]{1,0:T(8,128)(2,1)S(1)} %collective-permute-done.4.refs_0_), channel_id=1, source_target_pairs={{448,416},{480,448},{0,480},{32,0},{64,32},{96,64},{128,96},{449,4... | collective-permute-start | bytes 417800 | tf_op jit(solution)/shard_map/ppermute | solution.py:307
  39.0 0.7 copy-start.6
  41.0 10.0 %collective-permute-start.7 = (bf16[136,512]{1,0:T(8,128)(2,1)S(1)}, bf16[136,512]{1,0:T(8,128)(2,1)S(1)}, u32[]{:S(2)}, u32[]{:S(2)}) collective-permute-start(bf16[136,512]{1,0:T(8,128)(2,1)S(1)} %collective-permute-done.5.refs_1_), channel_id=1, source_target_pairs={{96,128},{128,160},{160,192},{192,224},{224,256},{256,288},{288,32... | collective-permute-start | bytes 417800 | tf_op jit(solution)/shard_map/ppermute | solution.py:311
  41.7 9.4 %collective-permute-start.8 = (bf16[136,512]{1,0:T(8,128)(2,1)S(1)}, bf16[136,512]{1,0:T(8,128)(2,1)S(1)}, u32[]{:S(2)}, u32[]{:S(2)}) collective-permute-start(bf16[136,512]{1,0:T(8,128)(2,1)S(1)} %collective-permute-done.6.refs_0_), channel_id=1, source_target_pairs={{416,384},{448,416},{480,448},{0,480},{32,0},{64,32},{96,64},{417,... | collective-permute-start | bytes 417800 | tf_op jit(solution)/shard_map/ppermute | solution.py:307
  50.0 1.0 copy-start.7
  51.0 8.0 %collective-permute-start.9 = (bf16[136,512]{1,0:T(8,128)(2,1)S(1)}, bf16[136,512]{1,0:T(8,128)(2,1)S(1)}, u32[]{:S(2)}, u32[]{:S(2)}) collective-permute-start(bf16[136,512]{1,0:T(8,128)(2,1)S(1)} %collective-permute-done.7.refs_1_), channel_id=1, source_target_pairs={{128,160},{160,192},{192,224},{224,256},{256,288},{288,320},{320,3... | collective-permute-start | bytes 417800 | tf_op jit(solution)/shard_map/ppermute | solution.py:311
  51.7 8.5 %collective-permute-start.10 = (bf16[136,512]{1,0:T(8,128)(2,1)S(1)}, bf16[136,512]{1,0:T(8,128)(2,1)S(1)}, u32[]{:S(2)}, u32[]{:S(2)}) collective-permute-start(bf16[136,512]{1,0:T(8,128)(2,1)S(1)} %collective-permute-done.8.refs_0_), channel_id=1, source_target_pairs={{384,352},{416,384},{448,416},{480,448},{0,480},{32,0},{64,32},{38... | collective-permute-start | bytes 417800 | tf_op jit(solution)/shard_map/ppermute | solution.py:307
  58.3 0.7 copy-start.4
  60.3 7.3 %collective-permute-start.11 = (bf16[136,512]{1,0:T(8,128)(2,1)S(1)}, bf16[136,512]{1,0:T(8,128)(2,1)S(1)}, u32[]{:S(2)}, u32[]{:S(2)}) collective-permute-start(bf16[136,512]{1,0:T(8,128)(2,1)S(1)} %collective-permute-done.9.refs_1_), channel_id=1, source_target_pairs={{160,192},{192,224},{224,256},{256,288},{288,320},{320,352},{352,3... | collective-permute-start | bytes 417800 | tf_op jit(solution)/shard_map/ppermute | solution.py:311
  60.9 7.6 %collective-permute-start.12 = (bf16[136,512]{1,0:T(8,128)(2,1)S(1)}, bf16[136,512]{1,0:T(8,128)(2,1)S(1)}, u32[]{:S(2)}, u32[]{:S(2)}) collective-permute-start(bf16[136,512]{1,0:T(8,128)(2,1)S(1)} %collective-permute-done.10.refs_0_), channel_id=1, source_target_pairs={{352,320},{384,352},{416,384},{448,416},{480,448},{0,480},{32,0},{... | collective-permute-start | bytes 417800 | tf_op jit(solution)/shard_map/ppermute | solution.py:307
  66.6 1.0 copy-start.5
  68.6 6.3 %collective-permute-start.13 = (bf16[136,512]{1,0:T(8,128)(2,1)S(1)}, bf16[136,512]{1,0:T(8,128)(2,1)S(1)}, u32[]{:S(2)}, u32[]{:S(2)}) collective-permute-start(bf16[136,512]{1,0:T(8,128)(2,1)S(1)} %collective-permute-done.11.refs_1_), channel_id=1, source_target_pairs={{192,224},{224,256},{256,288},{288,320},{320,352},{352,384},{384,4... | collective-permute-start | bytes 417800 | tf_op jit(solution)/shard_map/ppermute | solution.py:311
  69.2 7.6 %collective-permute-start.14 = (bf16[136,512]{1,0:T(8,128)(2,1)S(1)}, bf16[136,512]{1,0:T(8,128)(2,1)S(1)}, u32[]{:S(2)}, u32[]{:S(2)}) collective-permute-start(bf16[136,512]{1,0:T(8,128)(2,1)S(1)} %collective-permute-done.12.refs_0_), channel_id=1, source_target_pairs={{320,288},{352,320},{384,352},{416,384},{448,416},{480,448},{0,480... | collective-permute-start | bytes 417800 | tf_op jit(solution)/shard_map/ppermute | solution.py:307
  76.9 0.9 collective-permute-start.15
  77.8 9.0 %collective-permute-start.16 = (f32[80,512]{1,0:T(8,128)S(1)}, f32[80,512]{1,0:T(8,128)S(1)}, u32[]{:S(2)}, u32[]{:S(2)}) collective-permute-start(f32[80,512]{1,0:T(8,128)S(1)} %get-tuple-element.80), channel_id=1, source_target_pairs={{0,16},{16,0},{1,17},{17,1},{2,18},{18,2},{3,19},{19,3},{4,20},{20... | collective-permute-start | bytes 491528 | tf_op jit(solution)/shard_map/ppermute | solution.py:320
  186.1 27.4 %copy-start = (bf16[4,512,128]{2,1,0:T(8,128)(2,1)S(1)}, bf16[4,512,128]{2,1,0:T(8,128)(2,1)}, u32[]{:S(2)}) copy-start(bf16[4,512,128]{2,1,0:T(8,128)(2,1)} %weight_ref.1) | copy-start | bytes 1572868
  186.1 27.4 %copy-start.1 = (bf16[512,128]{1,0:T(8,128)(2,1)S(1)}, bf16[512,128]{1,0:T(8,128)(2,1)}, u32[]{:S(2)}) copy-start(bf16[512,128]{1,0:T(8,128)(2,1)} %shared_ref.1) | copy-start | bytes 393220
  213.5 32.4 %copy-start.3 = (f32[512,2]{0,1:T(2,128)S(1)}, f32[512,2]{0,1:T(2,128)}, u32[]{:S(2)}) copy-start(f32[512,2]{0,1:T(2,128)} %param.23) | copy-start | bytes 12292

commit v5 on v4

--- a/solution.py
+++ b/solution.py
@@ -294,13 +294,15 @@
     chip = z.reshape(1)
     for k in range(1, chips // 2 + 1):
         if k == 2:
-            up, down, before, local = lax.optimization_barrier((up, down, before, local))
+            down, before, local = lax.optimization_barrier((down, before, local))
         elif k == 5:
-            up, down, before, prepared = lax.optimization_barrier((up, down, before, prepared))
+            down, before, prepared = lax.optimization_barrier((down, before, prepared))
         elif k == 6:
-            up, down, before, up_weight = lax.optimization_barrier((up, down, before, up_weight))
-        elif k > 1:
-            up, down, before = lax.optimization_barrier((up, down, before))
+            down, before, up_weight = lax.optimization_barrier((down, before, up_weight))
+        elif 1 < k < chips // 2:
+            down, before = lax.optimization_barrier((down, before))
+        if k > 1:
+            up, before = lax.optimization_barrier((up, before))
         arrived, outs = [], state
         if k < chips // 2:
             back = [((i - k + 1) % chips, (i - k) % chips) for i in range(chips // 2 - 1)]

time: 248 us -> 245 us (0.988)
  starting transfers between devices: 62.5 us -> 70.2 us
  blocking collectives: 155 us -> 149 us
  waiting for transfers between devices: 10.7 us -> 7 us
    all_to_all x5, blocking collectives: 155 us -> 149 us  [exchange(): return lax.all_to_all(array, axis, split_axis=0, concat_axis=0, tiled=True)]
    ppermute x1, starting transfers between devices: 2.86 us -> 8.74 us  [shards(): lax.ppermute(query, 'c', ((0, 1), (1, 0)))]
    ppermute x7, waiting for transfers between devices: 9.66 us -> 3.97 us  [shards(): down = lax.ppermute(down, 'z', back)]
    unnamed x24 -> x26, local copies, waits for them, and re-layouts: 5.48 us -> 4.59 us
  transfers between devices with their start and end apart: 18 -> 18, of which waited for: 6 -> 7; matrix products, arithmetic and copies ran while one was open for 2% -> 2% of each run, Pallas kernels for 1% -> 1%
where the time goes in v5:
time: 245 us; the launch traced here: 244 us
  blocking collectives  149 us (61%)
  starting transfers between devices  70.2 us (29%)
  waiting for transfers between devices  7 us (3%)
  local copies, waits for them, and re-layouts  6.54 us (3%)
  Pallas kernels  6.39 us (3%)
  other arithmetic  4.49 us (2%)
    all_to_all x5, blocking collectives, exchange(): return lax.all_to_all(array, axis, split_axis=0, concat_axis=0, tiled=True)  149 us
    ppermute x7, starting transfers between devices, shards(): down = lax.ppermute(down, 'z', back)  43.6 us
    ppermute x1, starting transfers between devices, shards(): lax.ppermute(query, 'c', ((0, 1), (1, 0)))  8.74 us
    ppermute x1, starting transfers between devices, shards(): other = lax.ppermute(sent, 'c', ((0, 1), (1, 0)))  7.87 us
    pallas_call x16, Pallas kernels, call(): pl.pallas_call(kernel, out_shape=outs, in_specs=specs, out_specs=jax.tree...  6.39 us
    ppermute x8, starting transfers between devices, shards(): up = lax.ppermute(up, 'z', [(i, i + 1) for i in range(k - 1, chips - 1)])  5.96 us
  transfers between devices with their start and end apart: 18, of which 7 were waited for; matrix products, arithmetic and copies ran while one was open for 2% of the time, Pallas kernels for 1%

profile of v5, /device:TPU:1, one launch (start us, length us, event | category | flops | bytes accessed | tf_op | source)
XLA Modules:
  0.0 244.1 jit_solution(9234796745462762770)
XLA Ops:
  0.0 0.7 fusion.3
  0.7 0.8 multiply_bitcast_fusion
  1.6 8.7 %collective-permute-start.8 = (bf16[72,512]{1,0:T(8,128)(2,1)S(1)}, bf16[72,512]{1,0:T(8,128)(2,1)S(1)}, u32[]{:S(2)}, u32[]{:S(2)}) collective-permute-start(bf16[72,512]{1,0:T(8,128)(2,1)S(1)} %concatenate.22), channel_id=1, source_target_pairs={{0,16},{16,0},{1,17},{17,1},{2,18},{18,2},{3,19},{19,3},{4,20},{20... | collective-permute-start | bytes 221192 | tf_op jit(solution)/shard_map/ppermute | solution.py:279
  10.4 1.7 concatenate.21.block_ref
  12.1 5.8 %collective-permute-start.7 = (bf16[136,512]{1,0:T(8,128)(2,1)S(1)}, bf16[136,512]{1,0:T(8,128)(2,1)S(1)}, u32[]{:S(2)}, u32[]{:S(2)}) collective-permute-start(bf16[136,512]{1,0:T(8,128)(2,1)S(1)} %concatenate.21.block_ref), channel_id=1, source_target_pairs={{0,480},{32,0},{64,32},{96,64},{128,96},{160,128},{192,160},{1,481... | collective-permute-start | bytes 417800 | tf_op jit(solution)/shard_map/ppermute | solution.py:309
  17.9 1.3 maximum_bitcast_fusion
  19.5 1.6 pad_maximum_fusion
  21.0 0.6 shard_map.145
  21.6 4.0 %all-to-all-start = ((bf16[4,128,2048]{2,1,0:T(8,128)(2,1)}), bf16[4,128,2048]{2,1,0:T(8,128)(2,1)S(1)}, u32[]{:S(2)}, u32[]{:S(2)}) async-start(bf16[4,128,2048]{2,1,0:T(8,128)(2,1)} %pad_maximum_fusion), calls=%async_computation | async-start | bytes 4194304 | tf_op jit(solution)/shard_map/all_to_all | solution.py:248
  25.7 1.3 collective-permute-start
  26.9 2.0 collective-permute-done.refs_1_
  28.9 0.7 collective-permute-start.1
  29.6 7.9 %collective-permute-start.9 = (bf16[136,512]{1,0:T(8,128)(2,1)S(1)}, bf16[136,512]{1,0:T(8,128)(2,1)S(1)}, u32[]{:S(2)}, u32[]{:S(2)}) collective-permute-start(bf16[136,512]{1,0:T(8,128)(2,1)S(1)} %collective-permute-done.7.refs_0_), channel_id=1, source_target_pairs={{480,448},{0,480},{32,0},{64,32},{96,64},{128,96},{160,128},{481,4... | collective-permute-start | bytes 417800 | tf_op jit(solution)/shard_map/ppermute | solution.py:309
  37.6 0.7 collective-permute-start.2
  38.3 1.3 collective-permute-done.9.refs_0_
  39.6 6.2 %collective-permute-start.10 = (bf16[136,512]{1,0:T(8,128)(2,1)S(1)}, bf16[136,512]{1,0:T(8,128)(2,1)S(1)}, u32[]{:S(2)}, u32[]{:S(2)}) collective-permute-start(bf16[136,512]{1,0:T(8,128)(2,1)S(1)} %collective-permute-done.9.refs_0_), channel_id=1, source_target_pairs={{448,416},{480,448},{0,480},{32,0},{64,32},{96,64},{128,96},{449,4... | collective-permute-start | bytes 417800 | tf_op jit(solution)/shard_map/ppermute | solution.py:309
  45.8 0.7 collective-permute-start.3
  46.5 0.7 copy-done.6
  47.2 0.5 collective-permute-done.10.refs_0_
  47.8 5.3 %collective-permute-start.11 = (bf16[136,512]{1,0:T(8,128)(2,1)S(1)}, bf16[136,512]{1,0:T(8,128)(2,1)S(1)}, u32[]{:S(2)}, u32[]{:S(2)}) collective-permute-start(bf16[136,512]{1,0:T(8,128)(2,1)S(1)} %collective-permute-done.10.refs_0_), channel_id=1, source_target_pairs={{416,384},{448,416},{480,448},{0,480},{32,0},{64,32},{96,64},{417,... | collective-permute-start | bytes 417800 | tf_op jit(solution)/shard_map/ppermute | solution.py:309
  53.1 1.1 copy.17
  54.3 0.3 shard_map.149.targets_ref
  54.7 0.7 collective-permute-start.4
  55.4 1.0 copy-done.7
  56.3 6.3 %collective-permute-start.12 = (bf16[136,512]{1,0:T(8,128)(2,1)S(1)}, bf16[136,512]{1,0:T(8,128)(2,1)S(1)}, u32[]{:S(2)}, u32[]{:S(2)}) collective-permute-start(bf16[136,512]{1,0:T(8,128)(2,1)S(1)} %collective-permute-done.11.refs_0_), channel_id=1, source_target_pairs={{384,352},{416,384},{448,416},{480,448},{0,480},{32,0},{64,32},{38... | collective-permute-start | bytes 417800 | tf_op jit(solution)/shard_map/ppermute | solution.py:309
  62.6 0.7 collective-permute-start.5
  63.3 0.7 copy-done.4
  64.1 0.5 collective-permute-done.12.refs_0_
  64.6 6.0 %collective-permute-start.13 = (bf16[136,512]{1,0:T(8,128)(2,1)S(1)}, bf16[136,512]{1,0:T(8,128)(2,1)S(1)}, u32[]{:S(2)}, u32[]{:S(2)}) collective-permute-start(bf16[136,512]{1,0:T(8,128)(2,1)S(1)} %collective-permute-done.12.refs_0_), channel_id=1, source_target_pairs={{352,320},{384,352},{416,384},{448,416},{480,448},{0,480},{32,0},{... | collective-permute-start | bytes 417800 | tf_op jit(solution)/shard_map/ppermute | solution.py:309
  70.6 0.7 collective-permute-start.6
  71.3 1.0 copy-done.5
  72.3 0.3 collective-permute-done.13.refs_0_
  72.6 6.2 %collective-permute-start.15 = (bf16[136,512]{1,0:T(8,128)(2,1)S(1)}, bf16[136,512]{1,0:T(8,128)(2,1)S(1)}, u32[]{:S(2)}, u32[]{:S(2)}) collective-permute-start(bf16[136,512]{1,0:T(8,128)(2,1)S(1)} %collective-permute-done.13.refs_0_), channel_id=1, source_target_pairs={{320,288},{352,320},{384,352},{416,384},{448,416},{480,448},{0,480... | collective-permute-start | bytes 417800 | tf_op jit(solution)/shard_map/ppermute | solution.py:309
  78.9 0.7 collective-permute-start.14
  79.6 1.3 collective-permute-done.15.refs_0_
  80.8 0.2 shard_map.153
  81.1 7.9 %collective-permute-start.16 = (f32[80,512]{1,0:T(8,128)S(1)}, f32[80,512]{1,0:T(8,128)S(1)}, u32[]{:S(2)}, u32[]{:S(2)}) collective-permute-start(f32[80,512]{1,0:T(8,128)S(1)} %get-tuple-element.68), channel_id=1, source_target_pairs={{0,16},{16,0},{1,17},{17,1},{2,18},{18,2},{3,19},{19,3},{4,20},{20... | collective-permute-start | bytes 491528 | tf_op jit(solution)/shard_map/ppermute | solution.py:322
  89.0 1.0 collective-permute-done.16.other_ref
  90.1 23.4 %all_to_all.30 = bf16[16,64,512]{2,1,0:T(8,128)(2,1)S(1)} all-to-all(bf16[16,64,512]{2,1,0:T(8,128)(2,1)S(1)} %shard_map.155), channel_id=1, replica_groups=mesh['z'=16,'c'=2,'y'=4,'x'=4] {'y','x'}, dimensions={0} | all-to-all | bytes 2097152 | tf_op jit(solution)/shard_map/all_to_all | solution.py:248
  113.5 1.0 shard_map.156
  114.5 39.4 %all_to_all.31 = bf16[32,40,128]{2,1,0:T(8,128)(2,1)S(1)} all-to-all(bf16[32,40,128]{2,1,0:T(8,128)(2,1)S(1)} %bitcast.43), channel_id=1, replica_groups=mesh['z'=16,'c'=2,'y'=4,'x'=4] {'z','c'}, dimensions={0} | all-to-all | bytes 655360 | tf_op jit(solution)/shard_map/all_to_all | solution.py:248
  153.9 0.4 shard_map.157
  154.3 27.4 %all_to_all.32.rows_ref = bf16[16,448,128]{2,1,0:T(8,128)(2,1)S(1)} all-to-all(bf16[16,448,128]{2,1,0:T(8,128)(2,1)S(1)} %shard_map.157), channel_id=1, replica_groups=mesh['z'=16,'c'=2,'y'=4,'x'=4] {'y','x'}, dimensions={0} | all-to-all | bytes 3670016 | tf_op jit(solution)/shard_map/all_to_all | solution.py:248
  181.8 1.2 shard_map.158
  183.0 27.3 %all_to_all.33.hidden_ref = bf16[16,448,128]{2,1,0:T(8,128)(2,1)S(1)} all-to-all(bf16[16,448,128]{2,1,0:T(8,128)(2,1)S(1)} %shard_map.158), channel_id=1, replica_groups=mesh['z'=16,'c'=2,'y'=4,'x'=4] {'y','x'}, dimensions={0} | all-to-all | bytes 3670016 | tf_op jit(solution)/shard_map/all_to_all | solution.py:248
  210.3 1.0 shard_map.159
  211.3 31.4 %all_to_all.34 = bf16[32,40,128]{2,1,0:T(8,128)(2,1)S(1)} all-to-all(bf16[32,40,128]{2,1,0:T(8,128)(2,1)S(1)} %bitcast.45), channel_id=1, replica_groups=mesh['z'=16,'c'=2,'y'=4,'x'=4] {'z','c'}, dimensions={0} | all-to-all | bytes 655360 | tf_op jit(solution)/shard_map/all_to_all | solution.py:248
  242.7 1.4 shard_map.160
  (48 shorter events, 0.8 us)
Async XLA Ops:
  1.6 19.4 %collective-permute-start.8 = (bf16[72,512]{1,0:T(8,128)(2,1)S(1)}, bf16[72,512]{1,0:T(8,128)(2,1)S(1)}, u32[]{:S(2)}, u32[]{:S(2)}) collective-permute-start(bf16[72,512]{1,0:T(8,128)(2,1)S(1)} %concatenate.22), channel_id=1, source_target_pairs={{0,16},{16,0},{1,17},{17,1},{2,18},{18,2},{3,19},{19,3},{4,20},{20... | collective-permute-start | bytes 221192 | tf_op jit(solution)/shard_map/ppermute | solution.py:279
  12.1 9.5 %collective-permute-start.7 = (bf16[136,512]{1,0:T(8,128)(2,1)S(1)}, bf16[136,512]{1,0:T(8,128)(2,1)S(1)}, u32[]{:S(2)}, u32[]{:S(2)}) collective-permute-start(bf16[136,512]{1,0:T(8,128)(2,1)S(1)} %concatenate.21.block_ref), channel_id=1, source_target_pairs={{0,480},{32,0},{64,32},{96,64},{128,96},{160,128},{192,160},{1,481... | collective-permute-start | bytes 417800 | tf_op jit(solution)/shard_map/ppermute | solution.py:309
  17.9 1.4 copy-start.9
  17.9 1.4 copy-start.10
  21.6 43.0 %all-to-all-start = ((bf16[4,128,2048]{2,1,0:T(8,128)(2,1)}), bf16[4,128,2048]{2,1,0:T(8,128)(2,1)S(1)}, u32[]{:S(2)}, u32[]{:S(2)}) async-start(bf16[4,128,2048]{2,1,0:T(8,128)(2,1)} %pad_maximum_fusion), calls=%async_computation | async-start | bytes 4194304 | tf_op jit(solution)/shard_map/all_to_all | solution.py:248
  25.7 3.3 %collective-permute-start = (bf16[136,512]{1,0:T(8,128)(2,1)S(1)}, bf16[136,512]{1,0:T(8,128)(2,1)S(1)}, u32[]{:S(2)}, u32[]{:S(2)}) collective-permute-start(bf16[136,512]{1,0:T(8,128)(2,1)S(1)} %concatenate.21.block_ref), channel_id=1, source_target_pairs={{0,32},{32,64},{64,96},{96,128},{128,160},{160,192},{192,224},{224... | collective-permute-start | bytes 417800 | tf_op jit(solution)/shard_map/ppermute | solution.py:313
  28.9 8.6 %collective-permute-start.1 = (bf16[136,512]{1,0:T(8,128)(2,1)S(1)}, bf16[136,512]{1,0:T(8,128)(2,1)S(1)}, u32[]{:S(2)}, u32[]{:S(2)}) collective-permute-start(bf16[136,512]{1,0:T(8,128)(2,1)S(1)} %collective-permute-done.refs_1_), channel_id=1, source_target_pairs={{32,64},{64,96},{96,128},{128,160},{160,192},{192,224},{224,256},{... | collective-permute-start | bytes 417800 | tf_op jit(solution)/shard_map/ppermute | solution.py:313
  29.6 9.9 %collective-permute-start.9 = (bf16[136,512]{1,0:T(8,128)(2,1)S(1)}, bf16[136,512]{1,0:T(8,128)(2,1)S(1)}, u32[]{:S(2)}, u32[]{:S(2)}) collective-permute-start(bf16[136,512]{1,0:T(8,128)(2,1)S(1)} %collective-permute-done.7.refs_0_), channel_id=1, source_target_pairs={{480,448},{0,480},{32,0},{64,32},{96,64},{128,96},{160,128},{481,4... | collective-permute-start | bytes 417800 | tf_op jit(solution)/shard_map/ppermute | solution.py:309
  37.6 8.2 %collective-permute-start.2 = (bf16[136,512]{1,0:T(8,128)(2,1)S(1)}, bf16[136,512]{1,0:T(8,128)(2,1)S(1)}, u32[]{:S(2)}, u32[]{:S(2)}) collective-permute-start(bf16[136,512]{1,0:T(8,128)(2,1)S(1)} %collective-permute-done.1.refs_1_), channel_id=1, source_target_pairs={{64,96},{96,128},{128,160},{160,192},{192,224},{224,256},{256,288}... | collective-permute-start | bytes 417800 | tf_op jit(solution)/shard_map/ppermute | solution.py:313
  39.6 14.6 %copy-start.8 = (bf16[512,128]{1,0:T(8,128)(2,1)S(1)}, bf16[512,128]{1,0:T(8,128)(2,1)}, u32[]{:S(2)}) copy-start(bf16[512,128]{1,0:T(8,128)(2,1)} %param.19) | copy-start | bytes 393220
  39.6 14.7 %copy-start.11 = (bf16[2048]{0:T(1024)(128)(2,1)S(1)}, bf16[2048]{0:T(1024)(128)(2,1)}, u32[]{:S(2)}) copy-start(bf16[2048]{0:T(1024)(128)(2,1)} %param.21) | copy-start | bytes 12292
  39.6 14.7 %copy-start.2 = (s32[512,2]{0,1:T(2,128)S(1)}, s32[512,2]{0,1:T(2,128)}, u32[]{:S(2)}) copy-start(s32[512,2]{0,1:T(2,128)} %param.22) | copy-start | bytes 12292
  39.6 8.2 %collective-permute-start.10 = (bf16[136,512]{1,0:T(8,128)(2,1)S(1)}, bf16[136,512]{1,0:T(8,128)(2,1)S(1)}, u32[]{:S(2)}, u32[]{:S(2)}) collective-permute-start(bf16[136,512]{1,0:T(8,128)(2,1)S(1)} %collective-permute-done.9.refs_0_), channel_id=1, source_target_pairs={{448,416},{480,448},{0,480},{32,0},{64,32},{96,64},{128,96},{449,4... | collective-permute-start | bytes 417800 | tf_op jit(solution)/shard_map/ppermute | solution.py:309
  45.8 8.9 %collective-permute-start.3 = (bf16[136,512]{1,0:T(8,128)(2,1)S(1)}, bf16[136,512]{1,0:T(8,128)(2,1)S(1)}, u32[]{:S(2)}, u32[]{:S(2)}) collective-permute-start(bf16[136,512]{1,0:T(8,128)(2,1)S(1)} %collective-permute-done.2.refs_1_), channel_id=1, source_target_pairs={{96,128},{128,160},{160,192},{192,224},{224,256},{256,288},{288,32... | collective-permute-start | bytes 417800 | tf_op jit(solution)/shard_map/ppermute | solution.py:313
  46.5 0.7 copy-start.6
  47.8 8.6 %collective-permute-start.11 = (bf16[136,512]{1,0:T(8,128)(2,1)S(1)}, bf16[136,512]{1,0:T(8,128)(2,1)S(1)}, u32[]{:S(2)}, u32[]{:S(2)}) collective-permute-start(bf16[136,512]{1,0:T(8,128)(2,1)S(1)} %collective-permute-done.10.refs_0_), channel_id=1, source_target_pairs={{416,384},{448,416},{480,448},{0,480},{32,0},{64,32},{96,64},{417,... | collective-permute-start | bytes 417800 | tf_op jit(solution)/shard_map/ppermute | solution.py:309
  54.7 7.9 %collective-permute-start.4 = (bf16[136,512]{1,0:T(8,128)(2,1)S(1)}, bf16[136,512]{1,0:T(8,128)(2,1)S(1)}, u32[]{:S(2)}, u32[]{:S(2)}) collective-permute-start(bf16[136,512]{1,0:T(8,128)(2,1)S(1)} %collective-permute-done.3.refs_1_), channel_id=1, source_target_pairs={{128,160},{160,192},{192,224},{224,256},{256,288},{288,320},{320,3... | collective-permute-start | bytes 417800 | tf_op jit(solution)/shard_map/ppermute | solution.py:313
  55.3 1.0 copy-start.7
  56.3 8.3 %collective-permute-start.12 = (bf16[136,512]{1,0:T(8,128)(2,1)S(1)}, bf16[136,512]{1,0:T(8,128)(2,1)S(1)}, u32[]{:S(2)}, u32[]{:S(2)}) collective-permute-start(bf16[136,512]{1,0:T(8,128)(2,1)S(1)} %collective-permute-done.11.refs_0_), channel_id=1, source_target_pairs={{384,352},{416,384},{448,416},{480,448},{0,480},{32,0},{64,32},{38... | collective-permute-start | bytes 417800 | tf_op jit(solution)/shard_map/ppermute | solution.py:309
  62.6 8.0 %collective-permute-start.5 = (bf16[136,512]{1,0:T(8,128)(2,1)S(1)}, bf16[136,512]{1,0:T(8,128)(2,1)S(1)}, u32[]{:S(2)}, u32[]{:S(2)}) collective-permute-start(bf16[136,512]{1,0:T(8,128)(2,1)S(1)} %collective-permute-done.4.refs_1_), channel_id=1, source_target_pairs={{160,192},{192,224},{224,256},{256,288},{288,320},{320,352},{352,3... | collective-permute-start | bytes 417800 | tf_op jit(solution)/shard_map/ppermute | solution.py:313
  63.3 0.7 copy-start.4
  64.6 8.0 %collective-permute-start.13 = (bf16[136,512]{1,0:T(8,128)(2,1)S(1)}, bf16[136,512]{1,0:T(8,128)(2,1)S(1)}, u32[]{:S(2)}, u32[]{:S(2)}) collective-permute-start(bf16[136,512]{1,0:T(8,128)(2,1)S(1)} %collective-permute-done.12.refs_0_), channel_id=1, source_target_pairs={{352,320},{384,352},{416,384},{448,416},{480,448},{0,480},{32,0},{... | collective-permute-start | bytes 417800 | tf_op jit(solution)/shard_map/ppermute | solution.py:309
  70.6 8.3 %collective-permute-start.6 = (bf16[136,512]{1,0:T(8,128)(2,1)S(1)}, bf16[136,512]{1,0:T(8,128)(2,1)S(1)}, u32[]{:S(2)}, u32[]{:S(2)}) collective-permute-start(bf16[136,512]{1,0:T(8,128)(2,1)S(1)} %collective-permute-done.5.refs_1_), channel_id=1, source_target_pairs={{192,224},{224,256},{256,288},{288,320},{320,352},{352,384},{384,4... | collective-permute-start | bytes 417800 | tf_op jit(solution)/shard_map/ppermute | solution.py:313
  71.3 1.0 copy-start.5
  72.6 8.2 %collective-permute-start.15 = (bf16[136,512]{1,0:T(8,128)(2,1)S(1)}, bf16[136,512]{1,0:T(8,128)(2,1)S(1)}, u32[]{:S(2)}, u32[]{:S(2)}) collective-permute-start(bf16[136,512]{1,0:T(8,128)(2,1)S(1)} %collective-permute-done.13.refs_0_), channel_id=1, source_target_pairs={{320,288},{352,320},{384,352},{416,384},{448,416},{480,448},{0,480... | collective-permute-start | bytes 417800 | tf_op jit(solution)/shard_map/ppermute | solution.py:309
  78.9 2.2 collective-permute-start.14
  81.1 8.9 %collective-permute-start.16 = (f32[80,512]{1,0:T(8,128)S(1)}, f32[80,512]{1,0:T(8,128)S(1)}, u32[]{:S(2)}, u32[]{:S(2)}) collective-permute-start(f32[80,512]{1,0:T(8,128)S(1)} %get-tuple-element.68), channel_id=1, source_target_pairs={{0,16},{16,0},{1,17},{17,1},{2,18},{18,2},{3,19},{19,3},{4,20},{20... | collective-permute-start | bytes 491528 | tf_op jit(solution)/shard_map/ppermute | solution.py:322
  183.0 27.4 %copy-start = (bf16[4,512,128]{2,1,0:T(8,128)(2,1)S(1)}, bf16[4,512,128]{2,1,0:T(8,128)(2,1)}, u32[]{:S(2)}) copy-start(bf16[4,512,128]{2,1,0:T(8,128)(2,1)} %weight_ref.1) | copy-start | bytes 1572868
  183.0 27.4 %copy-start.1 = (bf16[512,128]{1,0:T(8,128)(2,1)S(1)}, bf16[512,128]{1,0:T(8,128)(2,1)}, u32[]{:S(2)}) copy-start(bf16[512,128]{1,0:T(8,128)(2,1)} %shared_ref.1) | copy-start | bytes 393220
  210.3 32.3 %copy-start.3 = (f32[512,2]{0,1:T(2,128)S(1)}, f32[512,2]{0,1:T(2,128)}, u32[]{:S(2)}) copy-start(f32[512,2]{0,1:T(2,128)} %param.23) | copy-start | bytes 12292
